TPU v7x, 256 devices: a whole 4x4x8 slice. The times are simulated.
256 devices in a mesh: kv: 32 (over z, y), tp: 8 (over x, core).
Axes of the slice: x: 4, y: 4, z: 8, core: 2. Of those that a mesh axis runs over, the one named last changes fastest.
Arguments:
- tokens: bfloat16 [32768, 1024], P('kv', 'tp'), may hold values from -6 to 6
- query_weight: bfloat16 [1024, 2048], P(None, 'tp'), may hold values from -0.1875 to 0.1875
- latent_weight: bfloat16 [1024, 128], replicated, may hold values from -0.1875 to 0.1875
- query_gain: float32 [128], replicated, may hold values from 0.5 to 1.5
- key_gain: float32 [128], replicated, may hold values from 0.5 to 1.5
- value_up: bfloat16 [16, 128, 64], P('tp'), may hold values from -0.5 to 0.5
- out_weight: bfloat16 [1024, 1024], P('tp'), may hold values from -0.25 to 0.25
- out_gain: float32 [1024], replicated, may hold values from 0.5 to 1.5
- chosen: int32 [256, 32], P('kv'), may hold values from -1 to 255, as said below
Outputs:
- mixed_out: bfloat16 [32768, 1024], P('kv', 'tp')
Inputs may be any that keep to these rules, and one draw needn't show every extreme that they name: Row b lists the key blocks chosen for query block b: entry 0 is b itself, then distinct blocks before b, then -1 in every unused place. Block j is held by index j // 8 of kv. All query blocks of one index of kv together choose at most 2 distinct blocks held by any one other index, and some pair of indices reaches that bound; blocks held by the same index are chosen freely.
All inputs are finite; a program needn't handle non-finite values.
Results may differ from a plain program's by a relative error of at most 0.02.
Values may be sent and summed in bfloat16 or wider, within the bound.
A program may use at most 64 MiB of HBM per device.

v0:
```python
import functools

import jax
import jax.numpy as jnp
from jax import lax
from jax.experimental import pallas as pl
from jax.experimental.pallas import tpu as pltpu
from jax.sharding import PartitionSpec as P

BLOCK = 128
PER_OWNER = 2
CHUNKS = 4
LAG = 2
MESH = pl.DeviceIdType.MESH

epsilon = 1e-06
masked_score = -1e30


def rms_scale(values, gain_row):
    widened = values.astype(jnp.float32)
    mean_sq = jnp.mean(widened * widened, axis=-1, keepdims=True)
    return (widened * lax.rsqrt(mean_sq + epsilon) * gain_row).astype(jnp.bfloat16)


def norm_keys(pool_ref, gain_ref, kn_ref, vx_ref, rows):
    lat = pool_ref[rows, :]
    kn_ref[rows, :] = rms_scale(lat, gain_ref[...])
    vx_ref[rows, 0:lat.shape[1]] = lat
    vx_ref[rows, lat.shape[1] :] = jnp.ones_like(lat)


def attend_block(b, own_pairs, q_ref, kn_ref, vx_ref, bias_ref, p_ref, vu_ref):
    width = kn_ref.shape[1]
    heads = q_ref.shape[1] // width
    pairs = kn_ref.shape[0] // (2 * BLOCK)
    rows = pl.ds(pl.multiple_of(b * BLOCK, BLOCK), BLOCK)
    q = jnp.concatenate([q_ref[rows, h * width : (h + 1) * width] for h in range(heads)], axis=0)
    shape = (heads * BLOCK, 2 * BLOCK)
    row_pos = lax.broadcasted_iota(jnp.int32, shape, 0) % BLOCK + b * BLOCK
    col_pos = lax.broadcasted_iota(jnp.int32, shape, 1)
    for i in range(pairs):
        cols = slice(i * 2 * BLOCK, (i + 1) * 2 * BLOCK)
        s = lax.dot_general(
            q, kn_ref[cols, :], (((1,), (1,)), ((), ())), preferred_element_type=jnp.float32
        )
        s = s + bias_ref[pl.ds(b, 1), cols]
        if i < own_pairs:
            s = jnp.where(col_pos + i * 2 * BLOCK <= row_pos, s, masked_score)
        p_ref[:, cols] = jnp.exp2(s).astype(jnp.bfloat16)
    acc = jnp.dot(p_ref[...], vx_ref[...], preferred_element_type=jnp.float32)
    att = (acc[:, :width] / acc[:, width:]).astype(jnp.bfloat16)
    out = []
    for h in range(0, heads, 2):
        two = jnp.concatenate(
            [att[h * BLOCK : (h + 1) * BLOCK], att[(h + 1) * BLOCK : (h + 2) * BLOCK]], axis=1
        )
        out.append(jnp.dot(two, vu_ref[h // 2], preferred_element_type=jnp.float32))
    return jnp.concatenate(out, axis=1).astype(jnp.bfloat16)


def paired_up(value_up):
    heads, width, vdim = value_up.shape
    pairs = value_up.reshape(heads // 2, 2, width, vdim)
    first = jnp.pad(pairs[:, 0], ((0, 0), (0, 0), (0, vdim)))
    second = jnp.pad(pairs[:, 1], ((0, 0), (0, 0), (vdim, 0)))
    return jnp.concatenate([first, second], axis=1)


def picked(table, first, count):
    found, rank = [], jnp.zeros((1, 1), jnp.float32)
    for j in range(count):
        rows = jnp.max(jnp.where(table == first + j, 1.0, 0.0), axis=1, keepdims=True)
        need = jnp.max(rows, axis=0, keepdims=True)
        found.append((rows, need, rank))
        rank = rank + need
    return found


def send(src, dst, sems, where):
    return pltpu.make_async_remote_copy(
        src_ref=src, dst_ref=dst, send_sem=sems[0], recv_sem=sems[1], device_id=where, device_id_type=MESH
    )


def kernel(
    kv_n, tp_n,
    tok_ref, wq_ref, wl_ref, qgain_ref, kgain_ref, vu_ref, w_ref, ogain_ref, chosen_ref,
    o_ref,
    tk_ref, q_ref, pool_ref, bias_ref, chs_ref, out_ref, kn_ref, vx_ref, p_ref,
    ho_ref, wc_ref, proj_ref, ss_ref, rs_ref,
    ch_s, ch_r, ts_s, ts_r, tx_s, tx_r, tr_s, tr_r, b_s, b_r, f_s, f_r,
    hs_s, hs_r, hx_s, hx_r, hr_s, hr_r, w_s, w_r, s_s, s_r,
):
    kv, tp = lax.axis_index("kv"), lax.axis_index("tp")
    core = lax.rem(tp, 2)
    sib = tp + 1 - 2 * core
    far = tp_n // 2 - 1
    toks, feat = tok_ref.shape
    width = wl_ref.shape[1]
    heads = wq_ref.shape[1] // width
    blocks = toks // BLOCK
    cols = o_ref.shape[1]
    crows = toks // CHUNKS

    def at_kv(other):
        return {"kv": other, "tp": tp}

    def at_tp(other):
        return {"kv": kv, "tp": other}

    def across(i, sign):
        return lax.rem(tp + sign * 2 * (i + 1) + tp_n, tp_n)

    barrier = pltpu.get_barrier_semaphore()
    for d in range(1, kv_n):
        pl.semaphore_signal(barrier, inc=1, device_id=at_kv(lax.rem(kv + d, kv_n)), device_id_type=MESH)
    for d in range(1, tp_n):
        pl.semaphore_signal(barrier, inc=1, device_id=at_tp(lax.rem(tp + d, tp_n)), device_id_type=MESH)
    pl.semaphore_wait(barrier, kv_n - 1 + tp_n - 1)

    def rows_of(c, n):
        return pl.ds(pl.multiple_of(c * n, n), n)

    def to_sib(src, buf, c, n, sems):
        return send(src.at[rows_of(c, n)], buf.at[tp, rows_of(c, n)], [s.at[c] for s in sems], at_tp(sib))

    def to_far(src, buf, c, n, i, sems):
        return send(
            src.at[rows_of(c, n)], buf.at[tp, rows_of(c, n)], [s.at[i, c] for s in sems], at_tp(across(i, 1))
        )

    def relay(buf, c, n, i, sems):
        part = buf.at[across(i, -1), rows_of(c, n)]
        return send(part, part, [s.at[i, c] for s in sems], at_tp(sib))

    def from_far(buf, c, n, i, sems):
        part = buf.at[across(i, -1), rows_of(c, n)]
        return send(part, part, [s.at[i, c] for s in sems], at_tp(sib))

    for c in range(CHUNKS):
        for i in range(far):
            to_far(tok_ref, tk_ref, c, crows, i, (tx_s, tx_r)).start()
        to_sib(tok_ref, tk_ref, c, crows, (ts_s, ts_r)).start()

    def ask(d):
        return send(chosen_ref, chs_ref.at[d - 1], (ch_s.at[d - 1], ch_r.at[d - 1]), at_kv(lax.rem(kv - d + kv_n, kv_n)))

    for d in range(1, kv_n):
        ask(d).start()

    tk_ref[tp] = tok_ref[...]
    table = chosen_ref[...]

    def put_bias(slot, hit):
        bias_ref[:, slot * BLOCK : (slot + 1) * BLOCK] = jnp.broadcast_to(
            (1.0 - hit) * masked_score, (blocks, BLOCK)
        )

    for j, (rows, _, _) in enumerate(picked(table, kv * blocks, blocks)):
        put_bias(j, rows)
    for d in range(1, kv_n):
        owner = kv - d
        first = jnp.where(owner >= 0, owner * blocks, -4 * blocks)
        found = picked(table, first, blocks)
        for k in range(PER_OWNER):
            hit = jnp.zeros((blocks, 1), jnp.float32)
            for rows, _, rank in found:
                hit = hit + jnp.where(rank == k, rows, 0.0)
            put_bias(blocks + (d - 1) * PER_OWNER + k, hit)

        @pl.when(owner < 0)
        def _(d=d):
            at = (blocks + (d - 1) * PER_OWNER) * BLOCK
            pool_ref[at : at + PER_OWNER * BLOCK, :] = jnp.zeros((PER_OWNER * BLOCK, width), jnp.bfloat16)

    gain = qgain_ref[...]

    def project(c):
        rows = slice(c * crows, (c + 1) * crows)
        x = jnp.concatenate([tk_ref[t, rows, :] for t in range(tp_n)], axis=1)
        lat = jnp.dot(x, wl_ref[...], preferred_element_type=jnp.float32)
        pool_ref[rows, :] = lat.astype(jnp.bfloat16)
        qs = jnp.dot(x, wq_ref[...], preferred_element_type=jnp.float32).astype(jnp.bfloat16)
        for h in range(heads):
            hc = slice(h * width, (h + 1) * width)
            q_ref[rows, hc] = rms_scale(qs[:, hc], gain)

    def arrive(c):
        to_sib(tok_ref, tk_ref, c, crows, (ts_s, ts_r)).wait()
        for i in range(far):
            relay(tk_ref, c, crows, i, (tr_s, tr_r)).wait()
            to_far(tok_ref, tk_ref, c, crows, i, (tx_s, tx_r)).wait_send()
        project(c)

    for c in range(CHUNKS):
        for i in range(far):
            from_far(tk_ref, c, crows, i, (tx_s, tx_r)).wait_recv()
            relay(tk_ref, c, crows, i, (tr_s, tr_r)).start()
        if c:
            arrive(c - 1)
    arrive(CHUNKS - 1)

    def weight(d):
        other = lax.rem(tp + d, tp_n)
        part = w_ref.at[:, pl.ds(pl.multiple_of(other * cols, cols), cols)]
        return send(part, wc_ref.at[tp], (w_s.at[d - 1], w_r.at[d - 1]), at_tp(other))

    def slot_rows(d, c):
        return pl.ds(pl.multiple_of((blocks + (d - 1) * PER_OWNER + c) * BLOCK, BLOCK), BLOCK)

    def give(d):
        return send(
            out_ref.at[d - 1], pool_ref.at[slot_rows(d, core)], (b_s.at[d - 1], b_r.at[d - 1]), at_kv(lax.rem(kv + d, kv_n))
        )

    def forward(d):
        part = pool_ref.at[slot_rows(d, core)]
        return send(part, part, (f_s.at[d - 1], f_r.at[d - 1]), at_tp(sib))

    mine = core.astype(jnp.float32)
    for d in range(1, kv_n):
        ask(d).wait()

        @pl.when(kv + d < kv_n)
        def _(d=d):
            total = jnp.zeros((BLOCK, width), jnp.float32)
            for j, (_, need, rank) in enumerate(picked(chs_ref[d - 1], kv * blocks, blocks)):
                share = jnp.where(rank == mine, need, 0.0)
                total = total + share * pool_ref[j * BLOCK : (j + 1) * BLOCK, :].astype(jnp.float32)
            out_ref[d - 1] = total.astype(jnp.bfloat16)
            give(d).start()

    for d in range(1, tp_n):
        weight(d).start()

    def norm(i):
        rows = pl.ds(pl.multiple_of(i * 2 * BLOCK, 2 * BLOCK), 2 * BLOCK)
        norm_keys(pool_ref, kgain_ref, kn_ref, vx_ref, rows)

    pl.loop(0, blocks // 2)(norm)
    wc_ref[tp] = w_ref[:, pl.ds(pl.multiple_of(tp * cols, cols), cols)]

    for d in range(1, kv_n):

        @pl.when(kv - d >= 0)
        def _(d=d):
            give(d).wait_recv()
            forward(d).start()

    for d in range(1, kv_n):

        @pl.when(kv - d >= 0)
        def _(d=d):
            forward(d).wait()

        norm(jnp.int32(blocks // 2 + d - 1))

    for d in range(1, kv_n):

        @pl.when(kv + d < kv_n)
        def _(d=d):
            give(d).wait_send()

    def hand_on(b):
        for i in range(far):
            from_far(ho_ref, b, BLOCK, i, (hx_s, hx_r)).wait_recv()
            relay(ho_ref, b, BLOCK, i, (hr_s, hr_r)).start()

    @pl.loop(0, blocks)
    def _(b):
        ho_ref[tp, rows_of(b, BLOCK), :] = attend_block(
            b, blocks // 2, q_ref, kn_ref, vx_ref, bias_ref, p_ref, vu_ref
        )
        for i in range(far):
            to_far(ho_ref.at[tp], ho_ref, b, BLOCK, i, (hx_s, hx_r)).start()
        to_sib(ho_ref.at[tp], ho_ref, b, BLOCK, (hs_s, hs_r)).start()

        @pl.when(b >= LAG)
        def _():
            hand_on(b - LAG)

    for d in range(1, tp_n):
        weight(d).wait()

    def finish(b):
        rows = rows_of(b, BLOCK)
        to_sib(ho_ref.at[tp], ho_ref, b, BLOCK, (hs_s, hs_r)).wait()
        for i in range(far):
            to_far(ho_ref.at[tp], ho_ref, b, BLOCK, i, (hx_s, hx_r)).wait_send()
            relay(ho_ref, b, BLOCK, i, (hr_s, hr_r)).wait()
        total = jnp.zeros((BLOCK, cols), jnp.float32)
        for t in range(tp_n):
            total = total + jnp.dot(ho_ref[t, rows, :], wc_ref[t], preferred_element_type=jnp.float32)
        proj_ref[rows, :] = total
        squares = jnp.sum(total * total, axis=1, keepdims=True)
        ss_ref[tp, pl.ds(b, 1), :] = jnp.broadcast_to(squares, (BLOCK, BLOCK)).T[0:1]

    for b in range(blocks - LAG, blocks):
        hand_on(b)
    pl.loop(0, blocks)(finish)

    def sums(d):
        return send(ss_ref.at[tp], ss_ref.at[tp], (s_s.at[d - 1], s_r.at[d - 1]), at_tp(lax.rem(tp + d, tp_n)))

    for d in range(1, tp_n):
        sums(d).start()
    for d in range(1, tp_n):
        sums(d).wait()
    total = ss_ref[0]
    for t in range(1, tp_n):
        total = total + ss_ref[t]
    rs_ref[...] = lax.rsqrt(total / (cols * tp_n) + epsilon)
    gains = ogain_ref[:, pl.ds(pl.multiple_of(tp * cols, cols), cols)]

    @pl.loop(0, blocks)
    def _(b):
        rows = rows_of(b, BLOCK)
        scale = jnp.broadcast_to(rs_ref[pl.ds(b, 1), :], (BLOCK, BLOCK)).T
        scale = jnp.concatenate([scale] * (cols // BLOCK), axis=1)
        o_ref[rows, :] = (proj_ref[rows, :] * scale * gains).astype(jnp.bfloat16)


def on_device(
    tokens,
    query_weight,
    latent_weight,
    query_gain,
    key_gain,
    value_up,
    out_weight,
    out_gain,
    chosen,
):
    toks, feat = tokens.shape
    width = latent_weight.shape[1]
    heads = query_weight.shape[1] // width
    blocks = toks // BLOCK
    kv_n, tp_n = lax.axis_size("kv"), lax.axis_size("tp")
    cols = out_weight.shape[1] // tp_n
    hv = out_weight.shape[0]
    far = tp_n // 2 - 1
    slots = blocks + (kv_n - 1) * PER_OWNER
    bf, f32 = jnp.bfloat16, jnp.float32
    wide = jnp.pad(chosen, ((0, 0), (0, BLOCK - chosen.shape[1])), constant_values=-1)
    scaled = (query_gain * (width**-0.5 * 1.4426950408889634))[None, :]
    dma = pltpu.SemaphoreType.DMA
    kvs, tps = [dma((kv_n - 1,))] * 2, [dma((tp_n - 1,))] * 2
    cs, cf = [dma((CHUNKS,))] * 2, [dma((far, CHUNKS))] * 2
    bs, bfar = [dma((blocks,))] * 2, [dma((far, blocks))] * 2
    return pl.pallas_call(
        functools.partial(kernel, kv_n, tp_n),
        out_shape=jax.ShapeDtypeStruct((toks, cols), bf),
        in_specs=[pl.BlockSpec(memory_space=pltpu.VMEM)] * 9,
        out_specs=pl.BlockSpec(memory_space=pltpu.VMEM),
        scratch_shapes=[
            pltpu.VMEM((tp_n, toks, feat), bf),
            pltpu.VMEM((toks, heads * width), bf),
            pltpu.VMEM((slots * BLOCK, width), bf),
            pltpu.VMEM((blocks, slots * BLOCK), f32),
            pltpu.VMEM((kv_n - 1, blocks, BLOCK), jnp.int32),
            pltpu.VMEM((kv_n - 1, BLOCK, width), bf),
            pltpu.VMEM((slots * BLOCK, width), bf),
            pltpu.VMEM((slots * BLOCK, 2 * width), bf),
            pltpu.VMEM((heads * BLOCK, slots * BLOCK), bf),
            pltpu.VMEM((tp_n, toks, hv), bf),
            pltpu.VMEM((tp_n, hv, cols), bf),
            pltpu.VMEM((toks, cols), f32),
            pltpu.VMEM((tp_n, blocks, BLOCK), f32),
            pltpu.VMEM((blocks, BLOCK), f32),
            *kvs, *cs, *cf, *cf, *kvs, *kvs, *bs, *bfar, *bfar, *tps, *tps,
        ],
        compiler_params=pltpu.CompilerParams(
            collective_id=0, has_side_effects=True, vmem_limit_bytes=60 << 20
        ),
    )(
        tokens, query_weight, latent_weight, scaled, key_gain[None, :], paired_up(value_up),
        out_weight, out_gain[None, :], wide,
    )


def solution(mesh):
    in_specs = (
        P("kv", "tp"),
        P(None, "tp"),
        P(),
        P(),
        P(),
        P("tp", None, None),
        P("tp", None),
        P(),
        P("kv", None),
    )
    out_specs = P("kv", "tp")
    return jax.shard_map(
        on_device, mesh=mesh, in_specs=in_specs, out_specs=out_specs, check_vma=False
    )
```

profile of v0, /device:TPU:201, one launch (start us, length us, event | category | flops | bytes accessed | tf_op | source)
XLA Modules:
  0.0 96.5 jit_solution(5625096696025599550)
XLA Ops:
  0.0 0.0 copy-start
  0.0 1.3 %multiply_bitcast_fusion.qgain_ref = f32[1,128]{1,0:T(1,128)} fusion(f32[128]{0:T(128)} %param.12), kind=kLoop, calls=%fused_computation.7 | loop fusion | flops 128 | bytes 1024 | tf_op jit(solution)/shard_map/broadcast_in_dim | solution.py:346
  1.3 0.0 copy-done
  1.3 0.6 pad.14.chosen_ref
  1.9 0.9 copy.10
  2.7 0.7 fusion.2.vu_ref
  3.5 91.3 %shard_map.91 = bf16[1024,128]{1,0:T(8,128)(2,1)} custom-call(bf16[1024,128]{1,0:T(8,128)(2,1)} %tok_ref.1, bf16[1024,256]{1,0:T(8,128)(2,1)} %wq_ref.1, bf16[1024,128]{1,0:T(8,128)(2,1)} %wl_ref.1, f32[1,128]{1,0:T(1,128)} %multiply_bitcast_fusion.qgain_ref, f32[1,128]{1,0:T(1,128)} %bitcast.11, bf16[1,256,128]{2,1,0:T(8,128)(2,1)} %fusion.2.vu_ref, ...), custom_call_target="tpu_custom_call" | custom-call | tf_op jit(solution)/shard_map/pallas_call | solution.py:351
  94.8 1.7 %copy.12 = bf16[1024,128]{1,0:T(8,128)(2,1)} copy(bf16[1024,128]{1,0:T(8,128)(2,1)} %shard_map.91) | data formatting | bytes 524288
  (1 shorter events, 0.0 us)
Async XLA Ops:
  0.0 1.3 %copy-start = (s32[8,32]{1,0:T(8,128)S(1)}, s32[8,32]{1,0:T(8,128)}, u32[]{:S(2)}) copy-start(s32[8,32]{1,0:T(8,128)} %param.17) | copy-start | bytes 3076
where the time goes:
time: 97.5 us; the launch traced here: 96.5 us
  Pallas kernels  91.3 us (94%)
  local copies, waits for them, and re-layouts  3.15 us (3%)
  other arithmetic  1.97 us (2%)
    pallas_call x1, Pallas kernels, on_device(): pl.pallas_call(functools.partial(kernel, kv_n, tp_n), out_shape=jax.Shape...  91.3 us
    unnamed x4, local copies, waits for them, and re-layouts  2.54 us

commit v1 on v0

v1 whole, which is shorter than its diff:
```python
import functools

import jax
import jax.numpy as jnp
from jax import lax
from jax.experimental import pallas as pl
from jax.experimental.pallas import tpu as pltpu
from jax.sharding import PartitionSpec as P

BLOCK = 128
PER_OWNER = 2
CHUNKS = 4
GROUP = 1
STEP = 8
LANES = 128
ONES = 16
MESH = pl.DeviceIdType.MESH

epsilon = 1e-06
masked_score = -1e30


def rms_scale(values, gain_row):
    widened = values.astype(jnp.float32)
    mean_sq = jnp.mean(widened * widened, axis=-1, keepdims=True)
    return (widened * lax.rsqrt(mean_sq + epsilon) * gain_row).astype(jnp.bfloat16)


def prefix_in_owner(values, lane, blocks, inclusive):
    total = values if inclusive else jnp.zeros_like(values)
    for s in range(1, blocks):
        total = total + jnp.where(lane % blocks >= s, pltpu.roll(values, s, 1), 0)
    return total


def send(src, dst, sems, where):
    return pltpu.make_async_remote_copy(
        src_ref=src, dst_ref=dst, send_sem=sems[0], recv_sem=sems[1], device_id=where, device_id_type=MESH
    )


def kernel(
    kv_n, tp_n,
    tok_ref, wq_ref, wl_ref, qgain_ref, kgain_ref, vu_ref, w_ref, ogain_ref, chosen_ref, chosen_s,
    o_ref,
    tk_ref, q_ref, own_ref, pool_ref, out_ref, kn_ref, vt_ref, bd_ref,
    map_ref, req_ref, chs_ref, map_s, chs_s,
    ho_ref, wc_ref, proj_ref, ss_ref, rs_ref,
    lc, ch_s, ch_r, ts_s, ts_r, tx_s, tx_r, tr_s, tr_r, b_s, b_r, f_s, f_r,
    hs_s, hs_r, hx_s, hx_r, hr_s, hr_r, w_s, w_r, s_s, s_r,
):
    kv, tp = lax.axis_index("kv"), lax.axis_index("tp")
    core = lax.rem(tp, 2)
    sib = tp + 1 - 2 * core
    far = tp_n // 2 - 1
    toks, feat = tok_ref.shape
    width = wl_ref.shape[1]
    heads = wq_ref.shape[1] // width
    vdim = vu_ref.shape[1]
    blocks = toks // BLOCK
    slots = blocks + pool_ref.shape[0]
    picks = chosen_ref.shape[1]
    cols = o_ref.shape[1]
    crows = toks // CHUNKS
    per_row = LANES // blocks

    def at_kv(other):
        return {"kv": other, "tp": tp}

    def at_tp(other):
        return {"kv": kv, "tp": other}

    def across(i, sign):
        return lax.rem(tp + sign * 2 * (i + 1) + tp_n, tp_n)

    barrier = pltpu.get_barrier_semaphore()
    for d in range(1, kv_n):
        pl.semaphore_signal(barrier, inc=1, device_id=at_kv(lax.rem(kv + d, kv_n)), device_id_type=MESH)
    for d in range(1, tp_n):
        pl.semaphore_signal(barrier, inc=1, device_id=at_tp(lax.rem(tp + d, tp_n)), device_id_type=MESH)

    lane = lax.broadcasted_iota(jnp.int32, (blocks, LANES), 1)
    halves = map_ref.shape[0]
    table = chosen_ref[...]
    for g in range(halves):
        hit = jnp.zeros((blocks, LANES), jnp.int32)
        for c in range(picks):
            hit = jnp.where(table[:, c : c + 1] == lane + g * LANES, 1, hit)
        need = jnp.broadcast_to(jnp.max(hit, axis=0, keepdims=True), (blocks, LANES))
        rank = prefix_in_owner(need, lane, blocks, False)
        local = lane % blocks
        dist = kv - (lane // blocks + g * per_row)
        slot = jnp.where(dist == 0, local, blocks + (dist - 1) * PER_OWNER + rank)
        map_ref[g] = jnp.clip(slot, 0, slots - 1)[0:1]
        code = jnp.zeros((blocks, LANES), jnp.int32)
        for k in range(PER_OWNER):
            code = code + jnp.where((need > 0) & (rank == k), local * blocks**k, 0)
        req_ref[g] = prefix_in_owner(code, lane, blocks, True)[0:1]

    pltpu.make_async_copy(map_ref, map_s, lc.at[0]).start()
    pl.semaphore_wait(barrier, kv_n - 1 + tp_n - 1)

    def rows_of(c, n):
        return pl.ds(pl.multiple_of(c * n, n), n)

    def to_sib(src, buf, c, n, sems):
        return send(src.at[rows_of(c, n)], buf.at[tp, rows_of(c, n)], [s.at[c] for s in sems], at_tp(sib))

    def to_far(src, buf, c, n, i, sems):
        return send(
            src.at[rows_of(c, n)], buf.at[tp, rows_of(c, n)], [s.at[i, c] for s in sems], at_tp(across(i, 1))
        )

    def relay(buf, c, n, i, sems):
        part = buf.at[across(i, -1), rows_of(c, n)]
        return send(part, part, [s.at[i, c] for s in sems], at_tp(sib))

    def from_far(buf, c, n, i, sems):
        part = buf.at[across(i, -1), rows_of(c, n)]
        return send(part, part, [s.at[i, c] for s in sems], at_tp(sib))

    for c in range(CHUNKS):
        for i in range(far):
            to_far(tok_ref, tk_ref, c, crows, i, (tx_s, tx_r)).start()
        to_sib(tok_ref, tk_ref, c, crows, (ts_s, ts_r)).start()

    def ask(d):
        owner = kv - d
        return send(
            req_ref.at[jnp.maximum(owner, 0) // per_row], chs_ref.at[d - 1],
            (ch_s.at[d - 1], ch_r.at[d - 1]), at_kv(lax.rem(owner + kv_n, kv_n)),
        )

    def asks(d):
        return kv - d >= 0

    def serves(d):
        return kv + d < kv_n

    for d in range(1, kv_n):

        @pl.when(asks(d))
        def _(d=d):
            ask(d).start()

    tk_ref[tp] = tok_ref[...]
    null = slots
    kn_ref[null] = jnp.zeros((BLOCK, width), jnp.bfloat16)
    vt_ref[null] = jnp.zeros((width + ONES, BLOCK), jnp.bfloat16)
    bd_ref[...] = jnp.zeros_like(bd_ref)
    for h in range(heads):
        bd_ref[h // 2, (h % 2) * vdim : (h % 2 + 1) * vdim, (h % 2) * width : (h % 2 + 1) * width] = vu_ref[h]

    gain = qgain_ref[...] * (width**-0.5 * 1.4426950408889634)

    def project(c):
        rows = slice(c * crows, (c + 1) * crows)
        x = jnp.concatenate([tk_ref[t, rows, :] for t in range(tp_n)], axis=1)
        lat = jnp.dot(x, wl_ref[...], preferred_element_type=jnp.float32).astype(jnp.bfloat16)
        for j in range(crows // BLOCK):
            own_ref[c * (crows // BLOCK) + j] = lat[j * BLOCK : (j + 1) * BLOCK]
        qs = jnp.dot(x, wq_ref[...], preferred_element_type=jnp.float32).astype(jnp.bfloat16)
        for h in range(heads):
            hc = slice(h * width, (h + 1) * width)
            q_ref[rows, hc] = rms_scale(qs[:, hc], gain)

    def arrive(c):
        to_sib(tok_ref, tk_ref, c, crows, (ts_s, ts_r)).wait()
        for i in range(far):
            relay(tk_ref, c, crows, i, (tr_s, tr_r)).wait()
            to_far(tok_ref, tk_ref, c, crows, i, (tx_s, tx_r)).wait_send()
        project(c)

    for c in range(CHUNKS):
        for i in range(far):
            from_far(tk_ref, c, crows, i, (tx_s, tx_r)).wait_recv()
            relay(tk_ref, c, crows, i, (tr_s, tr_r)).start()
        if c:
            arrive(c - 1)

    for d in range(1, kv_n):

        @pl.when(asks(d))
        def _(d=d):
            ask(d).wait_send()

        @pl.when(serves(d))
        def _(d=d):
            ask(d).wait_recv()

    pltpu.make_async_copy(map_ref, map_s, lc.at[0]).wait()
    to_smem = pltpu.make_async_copy(chs_ref, chs_s, lc.at[1])
    to_smem.start()
    arrive(CHUNKS - 1)
    to_smem.wait()

    def weight(d):
        other = lax.rem(tp + d, tp_n)
        part = w_ref.at[:, pl.ds(pl.multiple_of(other * cols, cols), cols)]
        return send(part, wc_ref.at[tp], (w_s.at[d - 1], w_r.at[d - 1]), at_tp(other))

    def slot_of(d, c):
        return (d - 1) * PER_OWNER + c

    def give(d):
        return send(
            out_ref.at[d - 1], pool_ref.at[slot_of(d, core)], (b_s.at[d - 1], b_r.at[d - 1]), at_kv(lax.rem(kv + d, kv_n))
        )

    def forward(d):
        part = pool_ref.at[slot_of(d, core)]
        return send(part, part, (f_s.at[d - 1], f_r.at[d - 1]), at_tp(sib))

    mine = lax.rem(kv, per_row) * blocks + blocks - 1
    for d in range(1, kv_n):

        @pl.when(serves(d))
        def _(d=d):
            code = chs_s[d - 1, 0, mine]
            want = jnp.where(core == 0, code, code >> 3) & (blocks - 1)
            out_ref[d - 1] = own_ref[want]
            give(d).start()

    for d in range(1, tp_n):
        weight(d).start()

    def norm(lat, slot):
        kn_ref[slot] = rms_scale(lat, kgain_ref[...])
        vt_ref[slot, 0:width, :] = lat.T
        vt_ref[slot, width:, :] = jnp.ones((ONES, BLOCK), jnp.bfloat16)

    @pl.loop(0, blocks)
    def _(b):
        norm(own_ref[b], b)

    wc_ref[tp] = w_ref[:, pl.ds(pl.multiple_of(tp * cols, cols), cols)]

    for d in range(1, kv_n):

        @pl.when(asks(d))
        def _(d=d):
            give(d).wait_recv()
            forward(d).start()

    for d in range(1, kv_n):

        @pl.when(asks(d))
        def _(d=d):
            forward(d).wait()
            for k in range(PER_OWNER):
                norm(pool_ref[slot_of(d, k)], blocks + slot_of(d, k))

    for d in range(1, kv_n):

        @pl.when(serves(d))
        def _(d=d):
            give(d).wait_send()

    def hand_on(b):
        for i in range(far):
            from_far(ho_ref, b, BLOCK, i, (hx_s, hx_r)).wait_recv()
            relay(ho_ref, b, BLOCK, i, (hr_s, hr_r)).start()

    def listed(b, c):
        block = chosen_s[b, c]
        known = jnp.maximum(block, 0)
        return jnp.where(block < 0, null, map_s[known >> 7, 0, known & (LANES - 1)])

    def attend_block(b):
        rows = rows_of(b, BLOCK)
        q = jnp.concatenate([q_ref[rows, h * width : (h + 1) * width] for h in range(heads)], axis=0)
        qt = q.T
        acc = jnp.zeros((width + ONES, heads * BLOCK), jnp.float32)
        for i in range(0, picks, STEP):
            at = [listed(b, i + k) for k in range(STEP)]
            keys = jnp.concatenate([kn_ref[s] for s in at], axis=0)
            s = jnp.dot(keys, qt, preferred_element_type=jnp.float32)
            if i == 0:
                key_row = lax.broadcasted_iota(jnp.int32, s.shape, 0)
                query_row = lax.broadcasted_iota(jnp.int32, s.shape, 1) % BLOCK
                s = jnp.where((key_row <= query_row) | (key_row >= BLOCK), s, masked_score)
            p = jnp.exp2(s).astype(jnp.bfloat16)
            values = jnp.concatenate([vt_ref[s] for s in at], axis=1)
            acc = acc + jnp.dot(values, p, preferred_element_type=jnp.float32)
        att = (acc[:width] / acc[width : width + 1]).astype(jnp.bfloat16).T
        out = []
        for h in range(0, heads, 2):
            two = jnp.concatenate([att[h * BLOCK : (h + 1) * BLOCK], att[(h + 1) * BLOCK : (h + 2) * BLOCK]], axis=1)
            out.append(
                lax.dot_general(two, bd_ref[h // 2], (((1,), (1,)), ((), ())), preferred_element_type=jnp.float32)
            )
        return jnp.concatenate(out, axis=1).astype(jnp.bfloat16)

    @pl.loop(0, blocks // GROUP)
    def _(g):
        done = [attend_block(g * GROUP + u) for u in range(GROUP)]
        for u in range(GROUP):
            b = g * GROUP + u
            ho_ref[tp, rows_of(b, BLOCK), :] = done[u]
            for i in range(far):
                to_far(ho_ref.at[tp], ho_ref, b, BLOCK, i, (hx_s, hx_r)).start()
            to_sib(ho_ref.at[tp], ho_ref, b, BLOCK, (hs_s, hs_r)).start()

        @pl.when(g >= 1)
        def _():
            for u in range(GROUP):
                hand_on((g - 1) * GROUP + u)

    for d in range(1, tp_n):
        weight(d).wait()

    def finish(b):
        rows = rows_of(b, BLOCK)
        to_sib(ho_ref.at[tp], ho_ref, b, BLOCK, (hs_s, hs_r)).wait()
        for i in range(far):
            to_far(ho_ref.at[tp], ho_ref, b, BLOCK, i, (hx_s, hx_r)).wait_send()
            relay(ho_ref, b, BLOCK, i, (hr_s, hr_r)).wait()
        total = jnp.zeros((BLOCK, cols), jnp.float32)
        for t in range(tp_n):
            total = total + jnp.dot(ho_ref[t, rows, :], wc_ref[t], preferred_element_type=jnp.float32)
        proj_ref[rows, :] = total
        squares = jnp.sum(total * total, axis=1, keepdims=True)
        ss_ref[tp, pl.ds(b, 1), :] = jnp.broadcast_to(squares, (BLOCK, BLOCK)).T[0:1]

    for b in range(blocks - GROUP, blocks):
        hand_on(b)
    pl.loop(0, blocks)(finish)

    def sums(d):
        return send(ss_ref.at[tp], ss_ref.at[tp], (s_s.at[d - 1], s_r.at[d - 1]), at_tp(lax.rem(tp + d, tp_n)))

    for d in range(1, tp_n):
        sums(d).start()
    for d in range(1, tp_n):
        sums(d).wait()
    total = ss_ref[0]
    for t in range(1, tp_n):
        total = total + ss_ref[t]
    rs_ref[...] = lax.rsqrt(total / (cols * tp_n) + epsilon)
    gains = ogain_ref[:, pl.ds(pl.multiple_of(tp * cols, cols), cols)]

    @pl.loop(0, blocks)
    def _(b):
        rows = rows_of(b, BLOCK)
        scale = jnp.broadcast_to(rs_ref[pl.ds(b, 1), :], (BLOCK, BLOCK)).T
        scale = jnp.concatenate([scale] * (cols // BLOCK), axis=1)
        o_ref[rows, :] = (proj_ref[rows, :] * scale * gains).astype(jnp.bfloat16)


def on_device(
    tokens,
    query_weight,
    latent_weight,
    query_gain,
    key_gain,
    value_up,
    out_weight,
    out_gain,
    chosen,
):
    toks, feat = tokens.shape
    width = latent_weight.shape[1]
    heads = query_weight.shape[1] // width
    blocks = toks // BLOCK
    kv_n, tp_n = lax.axis_size("kv"), lax.axis_size("tp")
    cols = out_weight.shape[1] // tp_n
    hv = out_weight.shape[0]
    far = tp_n // 2 - 1
    slots = blocks + (kv_n - 1) * PER_OWNER
    halves = kv_n * blocks // LANES
    bf, f32, i32 = jnp.bfloat16, jnp.float32, jnp.int32
    dma = pltpu.SemaphoreType.DMA
    kvs, tps = [dma((kv_n - 1,))] * 2, [dma((tp_n - 1,))] * 2
    cs, cf = [dma((CHUNKS,))] * 2, [dma((far, CHUNKS))] * 2
    bs, bfar = [dma((blocks,))] * 2, [dma((far, blocks))] * 2
    vmem = pl.BlockSpec(memory_space=pltpu.VMEM)
    return pl.pallas_call(
        functools.partial(kernel, kv_n, tp_n),
        out_shape=jax.ShapeDtypeStruct((toks, cols), bf),
        in_specs=[vmem] * 9 + [pl.BlockSpec(memory_space=pltpu.SMEM)],
        out_specs=vmem,
        scratch_shapes=[
            pltpu.VMEM((tp_n, toks, feat), bf),
            pltpu.VMEM((toks, heads * width), bf),
            pltpu.VMEM((blocks, BLOCK, width), bf),
            pltpu.VMEM((slots - blocks, BLOCK, width), bf),
            pltpu.VMEM((kv_n - 1, BLOCK, width), bf),
            pltpu.VMEM((slots + 1, BLOCK, width), bf),
            pltpu.VMEM((slots + 1, width + ONES, BLOCK), bf),
            pltpu.VMEM((heads // 2, 2 * hv // heads, 2 * width), bf),
            pltpu.VMEM((halves, 1, LANES), i32),
            pltpu.VMEM((halves, 1, LANES), i32),
            pltpu.VMEM((kv_n - 1, 1, LANES), i32),
            pltpu.SMEM((halves, 1, LANES), i32),
            pltpu.SMEM((kv_n - 1, 1, LANES), i32),
            pltpu.VMEM((tp_n, toks, hv), bf),
            pltpu.VMEM((tp_n, hv, cols), bf),
            pltpu.VMEM((toks, cols), f32),
            pltpu.VMEM((tp_n, blocks, BLOCK), f32),
            pltpu.VMEM((blocks, BLOCK), f32),
            dma((2,)), *kvs, *cs, *cf, *cf, *kvs, *kvs, *bs, *bfar, *bfar, *tps, *tps,
        ],
        compiler_params=pltpu.CompilerParams(
            collective_id=0, has_side_effects=True, vmem_limit_bytes=60 << 20
        ),
    )(
        tokens, query_weight, latent_weight, query_gain[None, :], key_gain[None, :],
        jnp.swapaxes(value_up, 1, 2), out_weight, out_gain[None, :], chosen, chosen,
    )


def solution(mesh):
    in_specs = (
        P("kv", "tp"),
        P(None, "tp"),
        P(),
        P(),
        P(),
        P("tp", None, None),
        P("tp", None),
        P(),
        P("kv", None),
    )
    out_specs = P("kv", "tp")
    return jax.shard_map(
        on_device, mesh=mesh, in_specs=in_specs, out_specs=out_specs, check_vma=False
    )
```

time: 97.5 us -> 91.5 us (0.938)
  Pallas kernels: 91.3 us -> 88.6 us
  other arithmetic: 1.97 us -> 0 us
  local copies, waits for them, and re-layouts: 3.15 us -> 1.67 us
    pallas_call x1, Pallas kernels: 91.3 us -> 88.6 us  [on_device(): pl.pallas_call(functools.partial(kernel, kv_n, tp_n), out_shape=jax.Shape...]
    broadcast_in_dim x1 -> x0, other arithmetic: 1.26 us -> none  [on_device(): scaled = (query_gain * (width ** (-0.5) * 1.4426950408889634))[None, :]]
    unnamed x4 -> x1, local copies, waits for them, and re-layouts: 2.54 us -> 1.67 us
where the time goes in v1:
time: 91.5 us; the launch traced here: 90.3 us
  Pallas kernels  88.6 us (97%)
  local copies, waits for them, and re-layouts  1.67 us (2%)
    pallas_call x1, Pallas kernels, on_device(): pl.pallas_call(functools.partial(kernel, kv_n, tp_n), out_shape=jax.Shape...  88.6 us

profile of v1, /device:TPU:201, one launch (start us, length us, event | category | flops | bytes accessed | tf_op | source)
XLA Modules:
  0.0 90.3 jit_solution(17834046561016856955)
XLA Ops:
  0.0 88.6 %shard_map.91 = bf16[1024,128]{1,0:T(8,128)(2,1)} custom-call(bf16[1024,128]{1,0:T(8,128)(2,1)} %tok_ref.1, bf16[1024,256]{1,0:T(8,128)(2,1)} %wq_ref.1, bf16[1024,128]{1,0:T(8,128)(2,1)} %wl_ref.1, f32[1,128]{1,0:T(1,128)} %bitcast.6, f32[1,128]{1,0:T(1,128)} %bitcast.7, bf16[2,64,128]{2,1,0:T(8,128)(2,1)} %bitcast.4, bf16[128,1024]{1,0:T(8,128)(2,1)} %w_ref.1, ...), custom_call_target="tpu_custom_call" | custom-call | tf_op jit(solution)/shard_map/pallas_call | solution.py:377
  88.6 1.7 %copy.11 = bf16[1024,128]{1,0:T(8,128)(2,1)} copy(bf16[1024,128]{1,0:T(8,128)(2,1)} %shard_map.91) | data formatting | bytes 524288

commit v2 on v1

v2 whole, which is shorter than its diff:
```python
import functools

import jax
import jax.numpy as jnp
from jax import lax
from jax.experimental import pallas as pl
from jax.experimental.pallas import tpu as pltpu
from jax.sharding import PartitionSpec as P

BLOCK = 128
PER_OWNER = 2
RING = 4
OWNERS = 8
STEP = 8
LANES = 128
ONES = 16
MESH = pl.DeviceIdType.MESH

epsilon = 1e-06
masked_score = -1e30


def rms_scale(values, gain_row):
    widened = values.astype(jnp.float32)
    mean_sq = jnp.mean(widened * widened, axis=-1, keepdims=True)
    return (widened * lax.rsqrt(mean_sq + epsilon) * gain_row).astype(jnp.bfloat16)


def prefix_in_owner(values, lane, blocks, inclusive):
    total = values if inclusive else jnp.zeros_like(values)
    for s in range(1, blocks):
        total = total + jnp.where(lane % blocks >= s, pltpu.roll(values, s, 1), 0)
    return total


def send(src, dst, sems, where):
    return pltpu.make_async_remote_copy(
        src_ref=src, dst_ref=dst, send_sem=sems[0], recv_sem=sems[1], device_id=where, device_id_type=MESH
    )


def owner_groups(kv_n):
    return [(d, min(d + OWNERS, kv_n)) for d in range(1, kv_n, OWNERS)]


def kernel(
    kv_n, tp_n,
    tok_ref, wq_ref, wl_ref, qgain_ref, kgain_ref, vu_ref, w_ref, ogain_ref, chosen_ref, chosen_s,
    o_ref,
    tk_ref, wqs_ref, vus_ref, q_ref, lat_ref, out_ref, kvp_ref, kn_ref, vt_ref, bd_ref,
    map_ref, req_ref, chs_ref, map_s, chs_s,
    ho_ref, wc_ref, proj_ref, px_ref, ss_ref,
    lc, t_s, t_r, c_s, c_r, ch_s, ch_r, b_s, b_r, k_s, k_r, kr_s, kr_r,
    w_s, w_r, y_s, y_r, h_s, h_r, p_s, p_r, s_s, s_r,
):
    kv, tp = lax.axis_index("kv"), lax.axis_index("tp")
    core, x = lax.rem(tp, 2), tp // 2
    sib = tp + 1 - 2 * core
    blocks, _, xs, piece, feat = tok_ref.shape
    far = xs - 1
    width = wl_ref.shape[1]
    heads = wq_ref.shape[1] // width
    vdim = vu_ref.shape[1]
    slots = kvp_ref.shape[1]
    picks = chosen_ref.shape[1]
    cols = o_ref.shape[1]
    half = BLOCK // 2
    mine = blocks * piece
    per_row = LANES // blocks
    wrows = w_ref.shape[0] // RING
    y = lax.rem(kv, RING)

    def at_kv(other):
        return {"kv": other, "tp": tp}

    def at_tp(other):
        return {"kv": kv, "tp": other}

    def other_tp(d):
        return lax.rem(tp + d + tp_n, tp_n)

    barrier = pltpu.get_barrier_semaphore()
    for d in range(1, kv_n):
        pl.semaphore_signal(barrier, inc=1, device_id=at_kv(lax.rem(kv + d, kv_n)), device_id_type=MESH)
    for d in range(1, tp_n):
        pl.semaphore_signal(barrier, inc=1, device_id=at_tp(other_tp(d)), device_id_type=MESH)

    lane = lax.broadcasted_iota(jnp.int32, (blocks, LANES), 1)
    halves = map_ref.shape[0]
    table = chosen_ref[...]
    for g in range(halves):
        hit = jnp.zeros((blocks, LANES), jnp.int32)
        for c in range(picks):
            hit = jnp.where(table[:, c : c + 1] == lane + g * LANES, 1, hit)
        need = jnp.broadcast_to(jnp.max(hit, axis=0, keepdims=True), (blocks, LANES))
        rank = prefix_in_owner(need, lane, blocks, False)
        local = lane % blocks
        dist = kv - (lane // blocks + g * per_row)
        slot = jnp.where(dist == 0, local, blocks + (dist - 1) * PER_OWNER + rank)
        map_ref[g] = jnp.clip(slot, 0, slots - 1)[0:1]
        code = jnp.zeros((blocks, LANES), jnp.int32)
        for k in range(PER_OWNER):
            code = code + jnp.where((need > 0) & (rank == k), local * blocks**k, 0)
        req_ref[g] = prefix_in_owner(code, lane, blocks, True)[0:1]

    pltpu.make_async_copy(map_ref, map_s, lc.at[0]).start()
    pl.semaphore_wait(barrier, kv_n - 1 + tp_n - 1)

    def tokens_to(d, j):
        other = other_tp(d)
        part = lax.rem(other // 2 + j, xs)
        return send(
            tok_ref.at[:, lax.rem(other, 2), part], tk_ref.at[tp, part], (t_s.at[j, d - 1], t_r.at[j, d - 1]), at_tp(other)
        )

    def ask(d):
        owner = kv - d
        return send(
            req_ref.at[jnp.maximum(owner, 0) // per_row], chs_ref.at[d - 1],
            (ch_s.at[d - 1], ch_r.at[d - 1]), at_kv(lax.rem(owner + kv_n, kv_n)),
        )

    def asks(d):
        return kv - d >= 0

    def serves(d):
        return kv + d < kv_n

    def weights_to(d):
        other = other_tp(d)
        part = w_ref.at[
            pl.ds(pl.multiple_of(y * wrows, wrows), wrows),
            pl.ds(pl.multiple_of(other // 2 * 2 * cols, 2 * cols), 2 * cols),
        ]
        return send(part, wc_ref.at[tp, y], (w_s.at[d - 1], w_r.at[d - 1]), at_tp(other))

    def weights_on(e):
        part = wc_ref.at[:, y]
        other = kv - y + lax.rem(y + e, RING)
        return send(part, part, (y_s.at[e - 1], y_r.at[e - 1]), at_kv(other))

    to_sib = [
        send(wq_ref, wqs_ref, (c_s.at[0], c_r.at[0]), at_tp(sib)),
        send(vu_ref, vus_ref, (c_s.at[1], c_r.at[1]), at_tp(sib)),
    ]

    for d in range(1, tp_n):
        tokens_to(d, 0).start()
    for d in range(1, kv_n):

        @pl.when(asks(d))
        def _(d=d):
            ask(d).start()

    for j in range(1, xs):
        for d in range(1, tp_n):
            tokens_to(d, j).start()
    for copy in to_sib:
        copy.start()
    for d in range(1, tp_n):
        weights_to(d).start()

    for p in range(xs):
        tk_ref[tp, p] = tok_ref[:, core, p]
    wc_ref[tp, y] = w_ref[
        pl.ds(pl.multiple_of(y * wrows, wrows), wrows), pl.ds(pl.multiple_of(x * 2 * cols, 2 * cols), 2 * cols)
    ]
    null = slots
    kn_ref[null] = jnp.zeros((BLOCK, width), jnp.bfloat16)
    vt_ref[null] = jnp.zeros((width + ONES, BLOCK), jnp.bfloat16)
    bd_ref[...] = jnp.zeros_like(bd_ref)

    def features(p):
        return jnp.concatenate([tk_ref[t, p].reshape(mine, feat) for t in range(tp_n)], axis=1)

    for d in range(1, tp_n):
        tokens_to(d, 0).wait_recv()
    lat = jnp.dot(features(x), wl_ref[...], preferred_element_type=jnp.float32).astype(jnp.bfloat16)
    lat_ref[...] = lat.reshape(blocks, piece, width)
    kvp_ref[tp, 0:blocks] = lat.reshape(blocks, piece, width)

    for d in range(1, kv_n):

        @pl.when(asks(d))
        def _(d=d):
            ask(d).wait_send()

        @pl.when(serves(d))
        def _(d=d):
            ask(d).wait_recv()

    to_smem = pltpu.make_async_copy(chs_ref, chs_s, lc.at[1])
    to_smem.start()
    pltpu.make_async_copy(map_ref, map_s, lc.at[0]).wait()
    to_smem.wait()

    def slots_of(d):
        return pl.ds(blocks + (d - 1) * PER_OWNER, PER_OWNER)

    def give(d):
        return send(
            out_ref.at[d - 1], kvp_ref.at[tp, slots_of(d)], (b_s.at[d - 1], b_r.at[d - 1]), at_kv(lax.rem(kv + d, kv_n))
        )

    at_lane = lax.rem(kv, per_row) * blocks + blocks - 1
    for d in range(1, kv_n):

        @pl.when(serves(d))
        def _(d=d):
            code = chs_s[d - 1, 0, at_lane]
            for k in range(PER_OWNER):
                out_ref[d - 1, k] = lat_ref[(code >> (3 * k)) & (blocks - 1)]
            give(d).start()

    remote = owner_groups(kv_n)
    groups = [(0, blocks)] + [
        (blocks + (a - 1) * PER_OWNER, (b - a) * PER_OWNER) for a, b in remote
    ]

    def spread(g, i):
        part = kvp_ref.at[tp, pl.ds(*groups[g])]
        where = sib if i == far else other_tp(2 * (i + 1))
        return send(part, part, (k_s.at[g, i], k_r.at[g, i]), at_tp(where))

    def relay(g, i):
        part = kvp_ref.at[other_tp(-2 * (i + 1)), pl.ds(*groups[g])]
        return send(part, part, (kr_s.at[g, i], kr_r.at[g, i]), at_tp(sib))

    def when_group(g, body):
        if g == 0:
            body()
        else:
            pl.when(kv >= remote[g - 1][0])(body)

    def spread_group(g):
        def body():
            if g:
                for d in range(*remote[g - 1]):

                    @pl.when(asks(d))
                    def _(d=d):
                        give(d).wait_recv()

            for i in range(far + 1):
                spread(g, i).start()

        when_group(g, body)

    def relay_group(g):
        def body():
            for i in range(far):
                spread(g, i).wait_recv()
                relay(g, i).start()

        when_group(g, body)

    gain_k = kgain_ref[...]

    def norm_group(g):
        def body():
            spread(g, far).wait_recv()
            for i in range(far):
                relay(g, i).wait_recv()

            @pl.loop(groups[g][0], groups[g][0] + groups[g][1])
            def _(slot):
                rows = jnp.concatenate(
                    [kvp_ref[p * 2 + c, slot] for c in range(2) for p in range(xs)], axis=0
                )
                kn_ref[slot] = rms_scale(rows, gain_k)
                vt_ref[slot, 0:width, :] = rows.T
                vt_ref[slot, width:, :] = jnp.ones((ONES, BLOCK), jnp.bfloat16)

        when_group(g, body)

    gain_q = qgain_ref[...] * (width**-0.5 * 1.4426950408889634)

    def project(j):
        for d in range(1, tp_n):
            if j:
                tokens_to(d, j).wait_recv()
        p = lax.rem(x + j, xs)
        rows = features(p)
        for w, at in ((wq_ref, core), (wqs_ref, 1 - core)):
            qs = jnp.dot(rows, w[...], preferred_element_type=jnp.float32).astype(jnp.bfloat16)
            for h in range(heads):
                part = rms_scale(qs[:, h * width : (h + 1) * width], gain_q)
                q_ref[at * heads + h, p] = part.reshape(blocks, piece, width)

    spread_group(0)
    for copy in to_sib:
        copy.wait()
    for v, at in ((vu_ref, core), (vus_ref, 1 - core)):
        for h in range(heads):
            bd_ref[at, h * vdim : (h + 1) * vdim, h * width : (h + 1) * width] = v[h]
    project(0)
    count = len(groups)
    for g in range(1, count):
        spread_group(g)
        relay_group(g - 1)
        if g < xs:
            project(g)
        if g >= 2:
            norm_group(g - 2)
    for j in range(count, xs):
        project(j)
    for d in range(1, tp_n):
        weights_to(d).wait_recv()
    for e in range(1, RING):
        weights_on(e).start()
    relay_group(count - 1)
    if count >= 2:
        norm_group(count - 2)
    norm_group(count - 1)

    def listed(b, c):
        block = chosen_s[b, c]
        known = jnp.maximum(block, 0)
        return jnp.where(block < 0, null, map_s[known >> 7, 0, known & (LANES - 1)])

    def attend_block(b):
        q = jnp.concatenate([q_ref[h, p, b] for h in range(2 * heads) for p in range(xs)], axis=0)
        qt = q.T
        acc = jnp.zeros((width + ONES, 2 * heads * half), jnp.float32)
        for i in range(0, picks, STEP):
            at = [listed(b, i + k) for k in range(STEP)]
            keys = jnp.concatenate([kn_ref[s] for s in at], axis=0)
            s = jnp.dot(keys, qt, preferred_element_type=jnp.float32)
            if i == 0:
                key_row = lax.broadcasted_iota(jnp.int32, s.shape, 0)
                query_row = lax.broadcasted_iota(jnp.int32, s.shape, 1) % half + core * half
                s = jnp.where((key_row <= query_row) | (key_row >= BLOCK), s, masked_score)
            p = jnp.exp2(s).astype(jnp.bfloat16)
            values = jnp.concatenate([vt_ref[s] for s in at], axis=1)
            acc = acc + jnp.dot(values, p, preferred_element_type=jnp.float32)
        att = (acc[:width] / acc[width : width + 1]).astype(jnp.bfloat16).T
        out = []
        for h in range(0, 2 * heads, 2):
            two = jnp.concatenate([att[h * half : (h + 1) * half], att[(h + 1) * half : (h + 2) * half]], axis=1)
            out.append(
                lax.dot_general(two, bd_ref[h // 2], (((1,), (1,)), ((), ())), preferred_element_type=jnp.float32)
            )
        return jnp.concatenate(out, axis=1).astype(jnp.bfloat16)

    def heads_to(b, i):
        part = ho_ref.at[x, b]
        return send(part, part, (h_s.at[b, i], h_r.at[b, i]), at_tp(other_tp(2 * (i + 1))))

    def finish(g):
        for u in range(2):
            for i in range(far):
                heads_to(2 * g + u, i).wait_recv()
        total = jnp.zeros((BLOCK, 2 * cols), jnp.float32)
        for p in range(xs):
            rows = ho_ref[p, pl.ds(2 * g, 2)].reshape(BLOCK, 2 * cols)
            w = jnp.concatenate([wc_ref[2 * p + c].reshape(RING * wrows, 2 * cols) for c in range(2)], axis=0)
            total = total + jnp.dot(rows, w, preferred_element_type=jnp.float32)
        left, right = total[:, :cols], total[:, cols:]
        px_ref[g] = jnp.where(core == 0, right, left)
        proj_ref[g, core] = jnp.where(core == 0, left, right)
        squares = jnp.sum(total * total, axis=1, keepdims=True)
        ss_ref[tp, pl.ds(g, 1), :] = jnp.broadcast_to(squares, (BLOCK, BLOCK)).T[0:1]
        swap(g).start()

    def swap(g):
        return send(px_ref.at[g], proj_ref.at[g, core], (p_s.at[g], p_r.at[g]), at_tp(sib))

    pairs = blocks // 2
    for e in range(1, RING):
        weights_on(e).wait_recv()

    @pl.loop(0, blocks)
    def _(b):
        ho_ref[x, b] = attend_block(b)
        for i in range(far):
            heads_to(b, i).start()

        @pl.when((b >= 5) & (lax.rem(b, 2) == 1))
        def _():
            finish((b - 5) // 2)

    for g in range(max(pairs - 2, 0), pairs):
        finish(g)

    def sums(d):
        return send(ss_ref.at[tp], ss_ref.at[tp], (s_s.at[d - 1], s_r.at[d - 1]), at_tp(other_tp(d)))

    for d in range(1, tp_n):
        sums(d).start()

    for d in range(1, tp_n):
        for j in range(xs):
            tokens_to(d, j).wait_send()
        weights_to(d).wait_send()
    for e in range(1, RING):
        weights_on(e).wait_send()
    for d in range(1, kv_n):

        @pl.when(serves(d))
        def _(d=d):
            give(d).wait_send()

    for g in range(count):

        def drain(g=g):
            for i in range(far + 1):
                spread(g, i).wait_send()
            for i in range(far):
                relay(g, i).wait_send()

        when_group(g, drain)

    @pl.loop(0, blocks)
    def _(b):
        for i in range(far):
            heads_to(b, i).wait_send()

    for g in range(pairs):
        swap(g).wait()
    for d in range(1, tp_n):
        sums(d).wait()
    gains = ogain_ref[:, pl.ds(pl.multiple_of(tp * cols, cols), cols)]
    for c in range(2):
        total = ss_ref[c]
        for p in range(1, xs):
            total = total + ss_ref[2 * p + c]
        inverse = lax.rsqrt(total / (cols * tp_n) + epsilon)
        for g in range(pairs):
            scale = jnp.broadcast_to(inverse[g : g + 1], (BLOCK, BLOCK)).T
            scale = jnp.concatenate([scale] * (cols // BLOCK), axis=1)
            rows = (proj_ref[g, c] * scale * gains).astype(jnp.bfloat16)
            for u in range(2):
                o_ref[pl.ds((2 * g + u) * BLOCK + c * half, half), :] = rows[u * half : (u + 1) * half]


def on_device(
    tokens,
    query_weight,
    latent_weight,
    query_gain,
    key_gain,
    value_up,
    out_weight,
    out_gain,
    chosen,
):
    toks, feat = tokens.shape
    width = latent_weight.shape[1]
    heads = query_weight.shape[1] // width
    blocks = toks // BLOCK
    kv_n, tp_n = lax.axis_size("kv"), lax.axis_size("tp")
    cols = out_weight.shape[1] // tp_n
    hv = out_weight.shape[0]
    xs = tp_n // 2
    far = xs - 1
    piece = BLOCK // tp_n
    slots = blocks + (kv_n - 1) * PER_OWNER
    halves = max(1, kv_n * blocks // LANES)
    count = 1 + len(owner_groups(kv_n))
    bf, f32, i32 = jnp.bfloat16, jnp.float32, jnp.int32
    dma = pltpu.SemaphoreType.DMA
    vmem = pl.BlockSpec(memory_space=pltpu.VMEM)
    sems = [
        (xs, tp_n - 1), (2,), (kv_n - 1,), (kv_n - 1,), (count, far + 1), (count, far),
        (tp_n - 1,), (RING - 1,), (blocks, far), (blocks // 2,), (tp_n - 1,),
    ]
    return pl.pallas_call(
        functools.partial(kernel, kv_n, tp_n),
        out_shape=jax.ShapeDtypeStruct((toks, cols), bf),
        in_specs=[vmem] * 9 + [pl.BlockSpec(memory_space=pltpu.SMEM)],
        out_specs=vmem,
        scratch_shapes=[
            pltpu.VMEM((tp_n, xs, blocks, piece, feat), bf),
            pltpu.VMEM(query_weight.shape, bf),
            pltpu.VMEM((value_up.shape[0], value_up.shape[2], value_up.shape[1]), bf),
            pltpu.VMEM((2 * heads, xs, blocks, piece, width), bf),
            pltpu.VMEM((blocks, piece, width), bf),
            pltpu.VMEM((kv_n - 1, PER_OWNER, piece, width), bf),
            pltpu.VMEM((tp_n, slots, piece, width), bf),
            pltpu.VMEM((slots + 1, BLOCK, width), bf),
            pltpu.VMEM((slots + 1, width + ONES, BLOCK), bf),
            pltpu.VMEM((2, hv, 2 * width), bf),
            pltpu.VMEM((halves, 1, LANES), i32),
            pltpu.VMEM((halves, 1, LANES), i32),
            pltpu.VMEM((kv_n - 1, 1, LANES), i32),
            pltpu.SMEM((halves, 1, LANES), i32),
            pltpu.SMEM((kv_n - 1, 1, LANES), i32),
            pltpu.VMEM((xs, blocks, BLOCK // 2, 2 * hv), bf),
            pltpu.VMEM((tp_n, RING, hv // RING, 2 * cols), bf),
            pltpu.VMEM((blocks // 2, 2, BLOCK, cols), f32),
            pltpu.VMEM((blocks // 2, BLOCK, cols), f32),
            pltpu.VMEM((tp_n, blocks // 2, BLOCK), f32),
            dma((2,)), *[dma(shape) for shape in sems for _ in range(2)],
        ],
        compiler_params=pltpu.CompilerParams(
            collective_id=0, has_side_effects=True, vmem_limit_bytes=60 << 20
        ),
    )(
        tokens.reshape(blocks, 2, xs, piece, feat), query_weight, latent_weight, query_gain[None, :],
        key_gain[None, :], jnp.swapaxes(value_up, 1, 2), out_weight, out_gain[None, :], chosen, chosen,
    )


def solution(mesh):
    in_specs = (
        P("kv", "tp"),
        P(None, "tp"),
        P(),
        P(),
        P(),
        P("tp", None, None),
        P("tp", None),
        P(),
        P("kv", None),
    )
    out_specs = P("kv", "tp")
    return jax.shard_map(
        on_device, mesh=mesh, in_specs=in_specs, out_specs=out_specs, check_vma=False
    )
```

time: 91.5 us -> 69.3 us (0.76)
  the two profiles are of different devices: /device:TPU:201 before, /device:TPU:193 now
where the time goes in v2:
time: 69.3 us; the launch traced here: 69.2 us
  Pallas kernels  67.5 us (97%)
  local copies, waits for them, and re-layouts  1.67 us (2%)
    pallas_call x1, Pallas kernels, on_device(): pl.pallas_call(functools.partial(kernel, kv_n, tp_n), out_shape=jax.Shape...  67.5 us
    unnamed x1, local copies, waits for them, and re-layouts  1.67 us

profile of v2, /device:TPU:193, one launch (start us, length us, event | category | flops | bytes accessed | tf_op | source)
XLA Modules:
  0.0 69.2 jit_solution(18242261518030103769)
XLA Ops:
  0.0 67.5 %shard_map.91 = bf16[1024,128]{1,0:T(8,128)(2,1)} custom-call(bf16[8,2,4,16,128]{4,3,2,1,0:T(8,128)(2,1)} %bitcast.5, bf16[1024,256]{1,0:T(8,128)(2,1)} %wq_ref.1, bf16[1024,128]{1,0:T(8,128)(2,1)} %wl_ref.1, f32[1,128]{1,0:T(1,128)} %bitcast.8, f32[1,128]{1,0:T(1,128)} %bitcast.9, bf16[2,64,128]{2,1,0:T(8,128)(2,1)} %bitcast.6, bf16[128,1024]{1,0:T(8,128)(2,1)} %w_ref.1, ...), custom_call_target="tpu_custom_call" | custom-call | tf_op jit(solution)/shard_map/pallas_call | solution.py:467
  67.5 1.7 %copy.11 = bf16[1024,128]{1,0:T(8,128)(2,1)} copy(bf16[1024,128]{1,0:T(8,128)(2,1)} %shard_map.91) | data formatting | bytes 524288

commit v3 on v2

--- a/solution.py
+++ b/solution.py
@@ -50,14 +50,13 @@
     tk_ref, wqs_ref, vus_ref, q_ref, lat_ref, out_ref, kvp_ref, kn_ref, vt_ref, bd_ref,
     map_ref, req_ref, chs_ref, map_s, chs_s,
     ho_ref, wc_ref, proj_ref, px_ref, ss_ref,
-    lc, t_s, t_r, c_s, c_r, ch_s, ch_r, b_s, b_r, k_s, k_r, kr_s, kr_r,
-    w_s, w_r, y_s, y_r, h_s, h_r, p_s, p_r, s_s, s_r,
+    lc, t_s, t_r, tf_s, tf_r, c_s, c_r, ch_s, ch_r, b_s, b_r, k_s, k_r, kf_s, kf_r, kr_s, kr_r,
+    w_s, w_r, y_s, y_r, h_s, h_r, hf_s, hf_r, p_s, p_r, s_s, s_r,
 ):
     kv, tp = lax.axis_index("kv"), lax.axis_index("tp")
     core, x = lax.rem(tp, 2), tp // 2
     sib = tp + 1 - 2 * core
     blocks, _, xs, piece, feat = tok_ref.shape
-    far = xs - 1
     width = wl_ref.shape[1]
     heads = wq_ref.shape[1] // width
     vdim = vu_ref.shape[1]
@@ -106,12 +105,25 @@
     pltpu.make_async_copy(map_ref, map_s, lc.at[0]).start()
     pl.semaphore_wait(barrier, kv_n - 1 + tp_n - 1)
 
-    def tokens_to(d, j):
-        other = other_tp(d)
-        part = lax.rem(other // 2 + j, xs)
+    def chip(i):
+        return lax.rem(x + i + xs, xs)
+
+    def same_core(i):
+        return 2 * chip(i) + core
+
+    def tokens_to(e, j):
+        c = lax.rem(core + e % 2, 2)
+        part = chip(e // 2 + j)
         return send(
-            tok_ref.at[:, lax.rem(other, 2), part], tk_ref.at[tp, part], (t_s.at[j, d - 1], t_r.at[j, d - 1]), at_tp(other)
+            tok_ref.at[:, c, part], tk_ref.at[tp, part], (t_s.at[j, e - 1], t_r.at[j, e - 1]), at_tp(2 * chip(e // 2) + c)
         )
+
+    beside = [e for e in range(1, tp_n) if e // 2 != 2]
+
+    def tokens_on(j, way):
+        step = 1 - 2 * way
+        part = tk_ref.at[2 * chip(-step) + way, chip(step + j)]
+        return send(part, part, (tf_s.at[j, way], tf_r.at[j, way]), at_tp(same_core(step)))
 
     def ask(d):
         owner = kv - d
@@ -144,8 +156,8 @@
         send(vu_ref, vus_ref, (c_s.at[1], c_r.at[1]), at_tp(sib)),
     ]
 
-    for d in range(1, tp_n):
-        tokens_to(d, 0).start()
+    for e in range(1, tp_n):
+        tokens_to(e, 0).start()
     for d in range(1, kv_n):
 
         @pl.when(asks(d))
@@ -153,8 +165,8 @@
             ask(d).start()
 
     for j in range(1, xs):
-        for d in range(1, tp_n):
-            tokens_to(d, j).start()
+        for e in beside:
+            tokens_to(e, j).start()
     for copy in to_sib:
         copy.start()
     for d in range(1, tp_n):
@@ -173,24 +185,34 @@
     def features(p):
         return jnp.concatenate([tk_ref[t, p].reshape(mine, feat) for t in range(tp_n)], axis=1)
 
-    for d in range(1, tp_n):
-        tokens_to(d, 0).wait_recv()
+    def hand_tokens(j):
+        if j:
+            for e in beside:
+                tokens_to(e, j).wait_recv()
+        if j != 1:
+            tokens_on((j - 1) % xs, 0).start()
+        if j < xs - 1:
+            tokens_on(j + 1, 1).start()
+
+    for d in range(1, kv_n):
+
+        @pl.when(asks(d))
+        def _(d=d):
+            ask(d).wait_send()
+
+        @pl.when(serves(d))
+        def _(d=d):
+            ask(d).wait_recv()
+
+    to_smem = pltpu.make_async_copy(chs_ref, chs_s, lc.at[1])
+    to_smem.start()
+    for e in range(1, tp_n):
+        tokens_to(e, 0).wait_recv()
+    hand_tokens(0)
     lat = jnp.dot(features(x), wl_ref[...], preferred_element_type=jnp.float32).astype(jnp.bfloat16)
     lat_ref[...] = lat.reshape(blocks, piece, width)
     kvp_ref[tp, 0:blocks] = lat.reshape(blocks, piece, width)
 
-    for d in range(1, kv_n):
-
-        @pl.when(asks(d))
-        def _(d=d):
-            ask(d).wait_send()
-
-        @pl.when(serves(d))
-        def _(d=d):
-            ask(d).wait_recv()
-
-    to_smem = pltpu.make_async_copy(chs_ref, chs_s, lc.at[1])
-    to_smem.start()
     pltpu.make_async_copy(map_ref, map_s, lc.at[0]).wait()
     to_smem.wait()
 
@@ -217,13 +239,26 @@
         (blocks + (a - 1) * PER_OWNER, (b - a) * PER_OWNER) for a, b in remote
     ]
 
+    def halves_of(g):
+        first, size = groups[g]
+        cut = (size + 1) // 2
+        return [pl.ds(first, cut), pl.ds(first + cut, size - cut)]
+
     def spread(g, i):
         part = kvp_ref.at[tp, pl.ds(*groups[g])]
-        where = sib if i == far else other_tp(2 * (i + 1))
+        where = sib if i == 2 else same_core(1 - 2 * i)
         return send(part, part, (k_s.at[g, i], k_r.at[g, i]), at_tp(where))
 
+    def pass_on(g, way):
+        step = 1 - 2 * way
+        part = kvp_ref.at[same_core(-step), halves_of(g)[way]]
+        return send(part, part, (kf_s.at[g, way], kf_r.at[g, way]), at_tp(same_core(step)))
+
     def relay(g, i):
-        part = kvp_ref.at[other_tp(-2 * (i + 1)), pl.ds(*groups[g])]
+        if i < 2:
+            part = kvp_ref.at[same_core(2 * i - 1), pl.ds(*groups[g])]
+        else:
+            part = kvp_ref.at[same_core(2), halves_of(g)[i - 2]]
         return send(part, part, (kr_s.at[g, i], kr_r.at[g, i]), at_tp(sib))
 
     def when_group(g, body):
@@ -241,16 +276,25 @@
                     def _(d=d):
                         give(d).wait_recv()
 
-            for i in range(far + 1):
+            for i in range(3):
                 spread(g, i).start()
+
+        when_group(g, body)
+
+    def pass_group(g):
+        def body():
+            for i in range(2):
+                spread(g, i).wait_recv()
+                pass_on(g, i).start()
+                relay(g, i).start()
 
         when_group(g, body)
 
     def relay_group(g):
         def body():
-            for i in range(far):
-                spread(g, i).wait_recv()
-                relay(g, i).start()
+            for i in range(2):
+                pass_on(g, i).wait_recv()
+                relay(g, i + 2).start()
 
         when_group(g, body)
 
@@ -258,8 +302,8 @@
 
     def norm_group(g):
         def body():
-            spread(g, far).wait_recv()
-            for i in range(far):
+            spread(g, 2).wait_recv()
+            for i in range(4):
                 relay(g, i).wait_recv()
 
             @pl.loop(groups[g][0], groups[g][0] + groups[g][1])
@@ -276,9 +320,9 @@
     gain_q = qgain_ref[...] * (width**-0.5 * 1.4426950408889634)
 
     def project(j):
-        for d in range(1, tp_n):
-            if j:
-                tokens_to(d, j).wait_recv()
+        if j:
+            for way in range(2):
+                tokens_on(j, way).wait_recv()
         p = lax.rem(x + j, xs)
         rows = features(p)
         for w, at in ((wq_ref, core), (wqs_ref, 1 - core)):
@@ -293,25 +337,25 @@
     for v, at in ((vu_ref, core), (vus_ref, 1 - core)):
         for h in range(heads):
             bd_ref[at, h * vdim : (h + 1) * vdim, h * width : (h + 1) * width] = v[h]
-    project(0)
     count = len(groups)
-    for g in range(1, count):
-        spread_group(g)
-        relay_group(g - 1)
-        if g < xs:
-            project(g)
-        if g >= 2:
-            norm_group(g - 2)
-    for j in range(count, xs):
-        project(j)
-    for d in range(1, tp_n):
-        weights_to(d).wait_recv()
-    for e in range(1, RING):
-        weights_on(e).start()
-    relay_group(count - 1)
-    if count >= 2:
-        norm_group(count - 2)
-    norm_group(count - 1)
+    for step in range(count + 3):
+        if step and step < count:
+            spread_group(step)
+        if 1 <= step <= count:
+            pass_group(step - 1)
+        if step + 1 < xs:
+            hand_tokens(step + 1)
+        if 2 <= step <= count + 1:
+            relay_group(step - 2)
+        if step < xs:
+            project(step)
+        if step >= 3:
+            norm_group(step - 3)
+        if step == 3:
+            for d in range(1, tp_n):
+                weights_to(d).wait_recv()
+            for e in range(1, RING):
+                weights_on(e).start()
 
     def listed(b, c):
         block = chosen_s[b, c]
@@ -342,14 +386,31 @@
             )
         return jnp.concatenate(out, axis=1).astype(jnp.bfloat16)
 
+    last = blocks - 1
+    pairs = blocks // 2
+
     def heads_to(b, i):
         part = ho_ref.at[x, b]
-        return send(part, part, (h_s.at[b, i], h_r.at[b, i]), at_tp(other_tp(2 * (i + 1))))
+        return send(part, part, (h_s.at[b, i], h_r.at[b, i]), at_tp(same_core((1, -1, 2)[i])))
+
+    def heads_on(b, way):
+        step = 1 - 2 * way
+        part = ho_ref.at[chip(-step), b, pl.ds(way * half // 2, half // 2)]
+        return send(part, part, (hf_s.at[b, way], hf_r.at[b, way]), at_tp(same_core(step)))
+
+    def pass_heads(b):
+        for way in range(2):
+            heads_to(b, way).wait_recv()
+            heads_on(b, way).start()
 
     def finish(g):
         for u in range(2):
-            for i in range(far):
-                heads_to(2 * g + u, i).wait_recv()
+            if not isinstance(g, jax.Array) and 2 * g + u == last:
+                for i in range(3):
+                    heads_to(last, i).wait_recv()
+            else:
+                for way in range(2):
+                    heads_on(2 * g + u, way).wait_recv()
         total = jnp.zeros((BLOCK, 2 * cols), jnp.float32)
         for p in range(xs):
             rows = ho_ref[p, pl.ds(2 * g, 2)].reshape(BLOCK, 2 * cols)
@@ -365,20 +426,30 @@
     def swap(g):
         return send(px_ref.at[g], proj_ref.at[g, core], (p_s.at[g], p_r.at[g]), at_tp(sib))
 
-    pairs = blocks // 2
-    for e in range(1, RING):
-        weights_on(e).wait_recv()
-
     @pl.loop(0, blocks)
     def _(b):
         ho_ref[x, b] = attend_block(b)
-        for i in range(far):
+        for i in range(2):
             heads_to(b, i).start()
+
+        @pl.when(b == last)
+        def _():
+            heads_to(last, 2).start()
+
+        @pl.when(b >= 2)
+        def _():
+            pass_heads(b - 2)
+
+        @pl.when(b == 4)
+        def _():
+            for e in range(1, RING):
+                weights_on(e).wait_recv()
 
         @pl.when((b >= 5) & (lax.rem(b, 2) == 1))
         def _():
             finish((b - 5) // 2)
 
+    pass_heads(last - 1)
     for g in range(max(pairs - 2, 0), pairs):
         finish(g)
 
@@ -388,9 +459,13 @@
     for d in range(1, tp_n):
         sums(d).start()
 
+    for j in range(xs):
+        for e in range(1, tp_n) if j == 0 else beside:
+            tokens_to(e, j).wait_send()
+        if j:
+            for way in range(2):
+                tokens_on(j, way).wait_send()
     for d in range(1, tp_n):
-        for j in range(xs):
-            tokens_to(d, j).wait_send()
         weights_to(d).wait_send()
     for e in range(1, RING):
         weights_on(e).wait_send()
@@ -403,18 +478,23 @@
     for g in range(count):
 
         def drain(g=g):
-            for i in range(far + 1):
+            for i in range(3):
                 spread(g, i).wait_send()
-            for i in range(far):
+            for i in range(2):
+                pass_on(g, i).wait_send()
+            for i in range(4):
                 relay(g, i).wait_send()
 
         when_group(g, drain)
 
-    @pl.loop(0, blocks)
+    @pl.loop(0, last)
     def _(b):
-        for i in range(far):
+        for i in range(2):
             heads_to(b, i).wait_send()
-
+            heads_on(b, i).wait_send()
+
+    for i in range(3):
+        heads_to(last, i).wait_send()
     for g in range(pairs):
         swap(g).wait()
     for d in range(1, tp_n):
@@ -452,7 +532,6 @@
     cols = out_weight.shape[1] // tp_n
     hv = out_weight.shape[0]
     xs = tp_n // 2
-    far = xs - 1
     piece = BLOCK // tp_n
     slots = blocks + (kv_n - 1) * PER_OWNER
     halves = max(1, kv_n * blocks // LANES)
@@ -461,8 +540,8 @@
     dma = pltpu.SemaphoreType.DMA
     vmem = pl.BlockSpec(memory_space=pltpu.VMEM)
     sems = [
-        (xs, tp_n - 1), (2,), (kv_n - 1,), (kv_n - 1,), (count, far + 1), (count, far),
-        (tp_n - 1,), (RING - 1,), (blocks, far), (blocks // 2,), (tp_n - 1,),
+        (xs, tp_n - 1), (xs, 2), (2,), (kv_n - 1,), (kv_n - 1,), (count, 3), (count, 2), (count, 4),
+        (tp_n - 1,), (RING - 1,), (blocks, 3), (blocks, 2), (blocks // 2,), (tp_n - 1,),
     ]
     return pl.pallas_call(
         functools.partial(kernel, kv_n, tp_n),

time: 69.3 us -> 71.9 us (1.038)
  the two profiles are of different devices: /device:TPU:193 before, /device:TPU:201 now
where the time goes in v3:
time: 71.9 us; the launch traced here: 71.4 us
  Pallas kernels  69.7 us (97%)
  local copies, waits for them, and re-layouts  1.67 us (2%)
    pallas_call x1, Pallas kernels, on_device(): pl.pallas_call(functools.partial(kernel, kv_n, tp_n), out_shape=jax.Shape...  69.7 us
    unnamed x1, local copies, waits for them, and re-layouts  1.67 us

profile of v3, /device:TPU:201, one launch (start us, length us, event | category | flops | bytes accessed | tf_op | source)
XLA Modules:
  0.0 71.4 jit_solution(4668518144664540603)
XLA Ops:
  0.0 69.7 %shard_map.91 = bf16[1024,128]{1,0:T(8,128)(2,1)} custom-call(bf16[8,2,4,16,128]{4,3,2,1,0:T(8,128)(2,1)} %bitcast.5, bf16[1024,256]{1,0:T(8,128)(2,1)} %wq_ref.1, bf16[1024,128]{1,0:T(8,128)(2,1)} %wl_ref.1, f32[1,128]{1,0:T(1,128)} %bitcast.8, f32[1,128]{1,0:T(1,128)} %bitcast.9, bf16[2,64,128]{2,1,0:T(8,128)(2,1)} %bitcast.6, bf16[128,1024]{1,0:T(8,128)(2,1)} %w_ref.1, ...), custom_call_target="tpu_custom_call" | custom-call | tf_op jit(solution)/shard_map/pallas_call | solution.py:546
  69.7 1.7 %copy.11 = bf16[1024,128]{1,0:T(8,128)(2,1)} copy(bf16[1024,128]{1,0:T(8,128)(2,1)} %shard_map.91) | data formatting | bytes 524288

commit v4 on v3

--- a/solution.py
+++ b/solution.py
@@ -46,12 +46,12 @@
 def kernel(
     kv_n, tp_n,
     tok_ref, wq_ref, wl_ref, qgain_ref, kgain_ref, vu_ref, w_ref, ogain_ref, chosen_ref, chosen_s,
-    o_ref,
-    tk_ref, wqs_ref, vus_ref, q_ref, lat_ref, out_ref, kvp_ref, kn_ref, vt_ref, bd_ref,
+    out_hbm,
+    o_ref, tk_ref, wqs_ref, vus_ref, q_ref, lat_ref, out_ref, kvp_ref, kn_ref, vt_ref, bd_ref,
     map_ref, req_ref, chs_ref, map_s, chs_s,
     ho_ref, wc_ref, proj_ref, px_ref, ss_ref,
-    lc, t_s, t_r, tf_s, tf_r, c_s, c_r, ch_s, ch_r, b_s, b_r, k_s, k_r, kf_s, kf_r, kr_s, kr_r,
-    w_s, w_r, y_s, y_r, h_s, h_r, hf_s, hf_r, p_s, p_r, s_s, s_r,
+    lc, oc, t_s, t_r, tf_s, tf_r, c_s, c_r, ch_s, ch_r, b_s, b_r, k_s, k_r, kf_s, kf_r, kr_s, kr_r,
+    w_s, w_r, y_s, y_r, h_s, h_r, p_s, p_r, s_s, s_r,
 ):
     kv, tp = lax.axis_index("kv"), lax.axis_index("tp")
     core, x = lax.rem(tp, 2), tp // 2
@@ -178,6 +178,7 @@
         pl.ds(pl.multiple_of(y * wrows, wrows), wrows), pl.ds(pl.multiple_of(x * 2 * cols, 2 * cols), 2 * cols)
     ]
     null = slots
+    vt_ref[:, width:, :] = jnp.ones((slots + 1, ONES, BLOCK), jnp.bfloat16)
     kn_ref[null] = jnp.zeros((BLOCK, width), jnp.bfloat16)
     vt_ref[null] = jnp.zeros((width + ONES, BLOCK), jnp.bfloat16)
     bd_ref[...] = jnp.zeros_like(bd_ref)
@@ -306,14 +307,18 @@
             for i in range(4):
                 relay(g, i).wait_recv()
 
-            @pl.loop(groups[g][0], groups[g][0] + groups[g][1])
-            def _(slot):
-                rows = jnp.concatenate(
-                    [kvp_ref[p * 2 + c, slot] for c in range(2) for p in range(xs)], axis=0
-                )
-                kn_ref[slot] = rms_scale(rows, gain_k)
-                vt_ref[slot, 0:width, :] = rows.T
-                vt_ref[slot, width:, :] = jnp.ones((ONES, BLOCK), jnp.bfloat16)
+            first, size = groups[g]
+            each = next(n for n in (4, 2, 1) if size % n == 0)
+
+            @pl.loop(0, size // each)
+            def _(i):
+                for u in range(each):
+                    slot = first + i * each + u
+                    rows = jnp.concatenate(
+                        [kvp_ref[p * 2 + c, slot] for c in range(2) for p in range(xs)], axis=0
+                    )
+                    kn_ref[slot] = rms_scale(rows, gain_k)
+                    vt_ref[slot, 0:width, :] = rows.T
 
         when_group(g, body)
 
@@ -338,17 +343,18 @@
         for h in range(heads):
             bd_ref[at, h * vdim : (h + 1) * vdim, h * width : (h + 1) * width] = v[h]
     count = len(groups)
-    for step in range(count + 3):
-        if step and step < count:
+    project(0)
+    for j in range(1, xs):
+        hand_tokens(j)
+    for step in range(1, count + 3):
+        if step < count:
             spread_group(step)
-        if 1 <= step <= count:
+        if step <= count:
             pass_group(step - 1)
-        if step + 1 < xs:
-            hand_tokens(step + 1)
         if 2 <= step <= count + 1:
             relay_group(step - 2)
-        if step < xs:
-            project(step)
+        if 2 <= step <= xs:
+            project(step - 1)
         if step >= 3:
             norm_group(step - 3)
         if step == 3:
@@ -386,31 +392,16 @@
             )
         return jnp.concatenate(out, axis=1).astype(jnp.bfloat16)
 
-    last = blocks - 1
     pairs = blocks // 2
 
     def heads_to(b, i):
         part = ho_ref.at[x, b]
-        return send(part, part, (h_s.at[b, i], h_r.at[b, i]), at_tp(same_core((1, -1, 2)[i])))
-
-    def heads_on(b, way):
-        step = 1 - 2 * way
-        part = ho_ref.at[chip(-step), b, pl.ds(way * half // 2, half // 2)]
-        return send(part, part, (hf_s.at[b, way], hf_r.at[b, way]), at_tp(same_core(step)))
-
-    def pass_heads(b):
-        for way in range(2):
-            heads_to(b, way).wait_recv()
-            heads_on(b, way).start()
+        return send(part, part, (h_s.at[b, i], h_r.at[b, i]), at_tp(same_core((2, 1, -1)[i])))
 
     def finish(g):
         for u in range(2):
-            if not isinstance(g, jax.Array) and 2 * g + u == last:
-                for i in range(3):
-                    heads_to(last, i).wait_recv()
-            else:
-                for way in range(2):
-                    heads_on(2 * g + u, way).wait_recv()
+            for i in range(3):
+                heads_to(2 * g + u, i).wait_recv()
         total = jnp.zeros((BLOCK, 2 * cols), jnp.float32)
         for p in range(xs):
             rows = ho_ref[p, pl.ds(2 * g, 2)].reshape(BLOCK, 2 * cols)
@@ -429,16 +420,8 @@
     @pl.loop(0, blocks)
     def _(b):
         ho_ref[x, b] = attend_block(b)
-        for i in range(2):
+        for i in range(3):
             heads_to(b, i).start()
-
-        @pl.when(b == last)
-        def _():
-            heads_to(last, 2).start()
-
-        @pl.when(b >= 2)
-        def _():
-            pass_heads(b - 2)
 
         @pl.when(b == 4)
         def _():
@@ -449,7 +432,6 @@
         def _():
             finish((b - 5) // 2)
 
-    pass_heads(last - 1)
     for g in range(max(pairs - 2, 0), pairs):
         finish(g)
 
@@ -487,30 +469,37 @@
 
         when_group(g, drain)
 
-    @pl.loop(0, last)
+    @pl.loop(0, blocks)
     def _(b):
-        for i in range(2):
+        for i in range(3):
             heads_to(b, i).wait_send()
-            heads_on(b, i).wait_send()
-
-    for i in range(3):
-        heads_to(last, i).wait_send()
+
     for g in range(pairs):
         swap(g).wait()
     for d in range(1, tp_n):
         sums(d).wait()
     gains = ogain_ref[:, pl.ds(pl.multiple_of(tp * cols, cols), cols)]
+    inverse = []
     for c in range(2):
         total = ss_ref[c]
         for p in range(1, xs):
             total = total + ss_ref[2 * p + c]
-        inverse = lax.rsqrt(total / (cols * tp_n) + epsilon)
-        for g in range(pairs):
-            scale = jnp.broadcast_to(inverse[g : g + 1], (BLOCK, BLOCK)).T
+        inverse.append(lax.rsqrt(total / (cols * tp_n) + epsilon))
+
+    def store(g):
+        part = pl.ds(2 * g * BLOCK, 2 * BLOCK)
+        return pltpu.make_async_copy(o_ref.at[part], out_hbm.at[part], oc.at[g])
+
+    for g in range(pairs):
+        for c in range(2):
+            scale = jnp.broadcast_to(inverse[c][g : g + 1], (BLOCK, BLOCK)).T
             scale = jnp.concatenate([scale] * (cols // BLOCK), axis=1)
             rows = (proj_ref[g, c] * scale * gains).astype(jnp.bfloat16)
             for u in range(2):
                 o_ref[pl.ds((2 * g + u) * BLOCK + c * half, half), :] = rows[u * half : (u + 1) * half]
+        store(g).start()
+    for g in range(pairs):
+        store(g).wait()
 
 
 def on_device(
@@ -541,14 +530,15 @@
     vmem = pl.BlockSpec(memory_space=pltpu.VMEM)
     sems = [
         (xs, tp_n - 1), (xs, 2), (2,), (kv_n - 1,), (kv_n - 1,), (count, 3), (count, 2), (count, 4),
-        (tp_n - 1,), (RING - 1,), (blocks, 3), (blocks, 2), (blocks // 2,), (tp_n - 1,),
+        (tp_n - 1,), (RING - 1,), (blocks, 3), (blocks // 2,), (tp_n - 1,),
     ]
     return pl.pallas_call(
         functools.partial(kernel, kv_n, tp_n),
         out_shape=jax.ShapeDtypeStruct((toks, cols), bf),
         in_specs=[vmem] * 9 + [pl.BlockSpec(memory_space=pltpu.SMEM)],
-        out_specs=vmem,
+        out_specs=pl.BlockSpec(memory_space=pl.ANY),
         scratch_shapes=[
+            pltpu.VMEM((toks, cols), bf),
             pltpu.VMEM((tp_n, xs, blocks, piece, feat), bf),
             pltpu.VMEM(query_weight.shape, bf),
             pltpu.VMEM((value_up.shape[0], value_up.shape[2], value_up.shape[1]), bf),
@@ -569,7 +559,7 @@
             pltpu.VMEM((blocks // 2, 2, BLOCK, cols), f32),
             pltpu.VMEM((blocks // 2, BLOCK, cols), f32),
             pltpu.VMEM((tp_n, blocks // 2, BLOCK), f32),
-            dma((2,)), *[dma(shape) for shape in sems for _ in range(2)],
+            dma((2,)), dma((blocks // 2,)), *[dma(shape) for shape in sems for _ in range(2)],
         ],
         compiler_params=pltpu.CompilerParams(
             collective_id=0, has_side_effects=True, vmem_limit_bytes=60 << 20

time: 71.9 us -> 65.5 us (0.911)
  Pallas kernels: 69.7 us -> 63.7 us
    pallas_call x1, Pallas kernels: 69.7 us -> 63.7 us  [on_device(): pl.pallas_call(functools.partial(kernel, kv_n, tp_n), out_shape=jax.Shape...]
where the time goes in v4:
time: 65.5 us; the launch traced here: 65.4 us
  Pallas kernels  63.7 us (97%)
  local copies, waits for them, and re-layouts  1.67 us (3%)
    pallas_call x1, Pallas kernels, on_device(): pl.pallas_call(functools.partial(kernel, kv_n, tp_n), out_shape=jax.Shape...  63.7 us
    unnamed x1, local copies, waits for them, and re-layouts  1.67 us

profile of v4, /device:TPU:201, one launch (start us, length us, event | category | flops | bytes accessed | tf_op | source)
XLA Modules:
  0.0 65.4 jit_solution(12833355354284670232)
XLA Ops:
  0.0 63.7 %shard_map.91 = bf16[1024,128]{1,0:T(8,128)(2,1)} custom-call(bf16[8,2,4,16,128]{4,3,2,1,0:T(8,128)(2,1)} %bitcast.5, bf16[1024,256]{1,0:T(8,128)(2,1)} %wq_ref.1, bf16[1024,128]{1,0:T(8,128)(2,1)} %wl_ref.1, f32[1,128]{1,0:T(1,128)} %bitcast.8, f32[1,128]{1,0:T(1,128)} %bitcast.9, bf16[2,64,128]{2,1,0:T(8,128)(2,1)} %bitcast.6, bf16[128,1024]{1,0:T(8,128)(2,1)} %w_ref.1, ...), custom_call_target="tpu_custom_call" | custom-call | tf_op jit(solution)/shard_map/pallas_call | solution.py:535
  63.7 1.7 %copy.11 = bf16[1024,128]{1,0:T(8,128)(2,1)} copy(bf16[1024,128]{1,0:T(8,128)(2,1)} %shard_map.91) | data formatting | bytes 524288

commit v5 on v4

--- a/solution.py
+++ b/solution.py
@@ -39,6 +39,10 @@
     )
 
 
+def arrived(part, sem):
+    pltpu.make_async_copy(part, part, sem).wait()
+
+
 def owner_groups(kv_n):
     return [(d, min(d + OWNERS, kv_n)) for d in range(1, kv_n, OWNERS)]
 
@@ -50,7 +54,7 @@
     o_ref, tk_ref, wqs_ref, vus_ref, q_ref, lat_ref, out_ref, kvp_ref, kn_ref, vt_ref, bd_ref,
     map_ref, req_ref, chs_ref, map_s, chs_s,
     ho_ref, wc_ref, proj_ref, px_ref, ss_ref,
-    lc, oc, t_s, t_r, tf_s, tf_r, c_s, c_r, ch_s, ch_r, b_s, b_r, k_s, k_r, kf_s, kf_r, kr_s, kr_r,
+    lc, oc, t_s, tf_s, t_r, tf_r, c_s, c_r, ch_s, ch_r, b_s, b_r, k_s, k_r, kf_r, kr_r,
     w_s, w_r, y_s, y_r, h_s, h_r, p_s, p_r, s_s, s_r,
 ):
     kv, tp = lax.axis_index("kv"), lax.axis_index("tp")
@@ -115,7 +119,7 @@
         c = lax.rem(core + e % 2, 2)
         part = chip(e // 2 + j)
         return send(
-            tok_ref.at[:, c, part], tk_ref.at[tp, part], (t_s.at[j, e - 1], t_r.at[j, e - 1]), at_tp(2 * chip(e // 2) + c)
+            tok_ref.at[:, c, part], tk_ref.at[tp, part], (t_s.at[j], t_r.at[j]), at_tp(2 * chip(e // 2) + c)
         )
 
     beside = [e for e in range(1, tp_n) if e // 2 != 2]
@@ -123,17 +127,14 @@
     def tokens_on(j, way):
         step = 1 - 2 * way
         part = tk_ref.at[2 * chip(-step) + way, chip(step + j)]
-        return send(part, part, (tf_s.at[j, way], tf_r.at[j, way]), at_tp(same_core(step)))
+        return send(part, part, (tf_s.at[0], tf_r.at[j]), at_tp(same_core(step)))
 
     def ask(d):
-        owner = kv - d
+        owner = lax.rem(kv - d + kv_n, kv_n)
         return send(
-            req_ref.at[jnp.maximum(owner, 0) // per_row], chs_ref.at[d - 1],
-            (ch_s.at[d - 1], ch_r.at[d - 1]), at_kv(lax.rem(owner + kv_n, kv_n)),
+            req_ref.at[owner // per_row], chs_ref.at[d - 1],
+            (ch_s.at[0], ch_r.at[0]), at_kv(owner),
         )
-
-    def asks(d):
-        return kv - d >= 0
 
     def serves(d):
         return kv + d < kv_n
@@ -144,12 +145,12 @@
             pl.ds(pl.multiple_of(y * wrows, wrows), wrows),
             pl.ds(pl.multiple_of(other // 2 * 2 * cols, 2 * cols), 2 * cols),
         ]
-        return send(part, wc_ref.at[tp, y], (w_s.at[d - 1], w_r.at[d - 1]), at_tp(other))
+        return send(part, wc_ref.at[tp, y], (w_s.at[0], w_r.at[0]), at_tp(other))
 
     def weights_on(e):
         part = wc_ref.at[:, y]
         other = kv - y + lax.rem(y + e, RING)
-        return send(part, part, (y_s.at[e - 1], y_r.at[e - 1]), at_kv(other))
+        return send(part, part, (y_s.at[0], y_r.at[0]), at_kv(other))
 
     to_sib = [
         send(wq_ref, wqs_ref, (c_s.at[0], c_r.at[0]), at_tp(sib)),
@@ -159,10 +160,7 @@
     for e in range(1, tp_n):
         tokens_to(e, 0).start()
     for d in range(1, kv_n):
-
-        @pl.when(asks(d))
-        def _(d=d):
-            ask(d).start()
+        ask(d).start()
 
     for j in range(1, xs):
         for e in beside:
@@ -188,27 +186,16 @@
 
     def hand_tokens(j):
         if j:
-            for e in beside:
-                tokens_to(e, j).wait_recv()
+            arrived(tk_ref.at[pl.ds(0, len(beside)), 0], t_r.at[j])
         if j != 1:
             tokens_on((j - 1) % xs, 0).start()
         if j < xs - 1:
             tokens_on(j + 1, 1).start()
 
-    for d in range(1, kv_n):
-
-        @pl.when(asks(d))
-        def _(d=d):
-            ask(d).wait_send()
-
-        @pl.when(serves(d))
-        def _(d=d):
-            ask(d).wait_recv()
-
+    arrived(chs_ref, ch_r.at[0])
     to_smem = pltpu.make_async_copy(chs_ref, chs_s, lc.at[1])
     to_smem.start()
-    for e in range(1, tp_n):
-        tokens_to(e, 0).wait_recv()
+    arrived(tk_ref.at[pl.ds(0, tp_n - 1), 0], t_r.at[0])
     hand_tokens(0)
     lat = jnp.dot(features(x), wl_ref[...], preferred_element_type=jnp.float32).astype(jnp.bfloat16)
     lat_ref[...] = lat.reshape(blocks, piece, width)
@@ -222,7 +209,7 @@
 
     def give(d):
         return send(
-            out_ref.at[d - 1], kvp_ref.at[tp, slots_of(d)], (b_s.at[d - 1], b_r.at[d - 1]), at_kv(lax.rem(kv + d, kv_n))
+            out_ref.at[d - 1], kvp_ref.at[tp, slots_of(d)], (b_s.at[0], b_r.at[(d - 1) // OWNERS]), at_kv(lax.rem(kv + d, kv_n))
         )
 
     at_lane = lax.rem(kv, per_row) * blocks + blocks - 1
@@ -248,19 +235,19 @@
     def spread(g, i):
         part = kvp_ref.at[tp, pl.ds(*groups[g])]
         where = sib if i == 2 else same_core(1 - 2 * i)
-        return send(part, part, (k_s.at[g, i], k_r.at[g, i]), at_tp(where))
+        return send(part, part, (k_s.at[g], (kr_r if i == 2 else k_r).at[g]), at_tp(where))
 
     def pass_on(g, way):
         step = 1 - 2 * way
         part = kvp_ref.at[same_core(-step), halves_of(g)[way]]
-        return send(part, part, (kf_s.at[g, way], kf_r.at[g, way]), at_tp(same_core(step)))
+        return send(part, part, (k_s.at[g], kf_r.at[g]), at_tp(same_core(step)))
 
     def relay(g, i):
         if i < 2:
             part = kvp_ref.at[same_core(2 * i - 1), pl.ds(*groups[g])]
         else:
             part = kvp_ref.at[same_core(2), halves_of(g)[i - 2]]
-        return send(part, part, (kr_s.at[g, i], kr_r.at[g, i]), at_tp(sib))
+        return send(part, part, (k_s.at[g], kr_r.at[g]), at_tp(sib))
 
     def when_group(g, body):
         if g == 0:
@@ -271,11 +258,12 @@
     def spread_group(g):
         def body():
             if g:
-                for d in range(*remote[g - 1]):
-
-                    @pl.when(asks(d))
-                    def _(d=d):
-                        give(d).wait_recv()
+                a, b = remote[g - 1]
+                for n in range(1, b - a + 1):
+
+                    @pl.when((kv >= b - 1) if n == b - a else (kv == a + n - 1))
+                    def _(n=n):
+                        arrived(kvp_ref.at[tp, pl.ds(groups[g][0], n * PER_OWNER)], b_r.at[g - 1])
 
             for i in range(3):
                 spread(g, i).start()
@@ -284,8 +272,8 @@
 
     def pass_group(g):
         def body():
+            arrived(kvp_ref.at[pl.ds(0, 2), pl.ds(*groups[g])], k_r.at[g])
             for i in range(2):
-                spread(g, i).wait_recv()
                 pass_on(g, i).start()
                 relay(g, i).start()
 
@@ -293,8 +281,8 @@
 
     def relay_group(g):
         def body():
+            arrived(kvp_ref.at[0, pl.ds(*groups[g])], kf_r.at[g])
             for i in range(2):
-                pass_on(g, i).wait_recv()
                 relay(g, i + 2).start()
 
         when_group(g, body)
@@ -303,9 +291,7 @@
 
     def norm_group(g):
         def body():
-            spread(g, 2).wait_recv()
-            for i in range(4):
-                relay(g, i).wait_recv()
+            arrived(kvp_ref.at[pl.ds(0, 4), pl.ds(*groups[g])], kr_r.at[g])
 
             first, size = groups[g]
             each = next(n for n in (4, 2, 1) if size % n == 0)
@@ -326,8 +312,7 @@
 
     def project(j):
         if j:
-            for way in range(2):
-                tokens_on(j, way).wait_recv()
+            arrived(tk_ref.at[pl.ds(0, 2), 0], tf_r.at[j])
         p = lax.rem(x + j, xs)
         rows = features(p)
         for w, at in ((wq_ref, core), (wqs_ref, 1 - core)):
@@ -358,8 +343,7 @@
         if step >= 3:
             norm_group(step - 3)
         if step == 3:
-            for d in range(1, tp_n):
-                weights_to(d).wait_recv()
+            arrived(wc_ref.at[pl.ds(0, tp_n - 1), 0], w_r.at[0])
             for e in range(1, RING):
                 weights_on(e).start()
 
@@ -396,12 +380,10 @@
 
     def heads_to(b, i):
         part = ho_ref.at[x, b]
-        return send(part, part, (h_s.at[b, i], h_r.at[b, i]), at_tp(same_core((2, 1, -1)[i])))
+        return send(part, part, (h_s.at[0], h_r.at[b // 2]), at_tp(same_core((2, 1, -1)[i])))
 
     def finish(g):
-        for u in range(2):
-            for i in range(3):
-                heads_to(2 * g + u, i).wait_recv()
+        arrived(ho_ref.at[pl.ds(0, xs - 1), pl.ds(0, 2)], h_r.at[g])
         total = jnp.zeros((BLOCK, 2 * cols), jnp.float32)
         for p in range(xs):
             rows = ho_ref[p, pl.ds(2 * g, 2)].reshape(BLOCK, 2 * cols)
@@ -415,7 +397,7 @@
         swap(g).start()
 
     def swap(g):
-        return send(px_ref.at[g], proj_ref.at[g, core], (p_s.at[g], p_r.at[g]), at_tp(sib))
+        return send(px_ref.at[g], proj_ref.at[g, core], (p_s.at[0], p_r.at[0]), at_tp(sib))
 
     @pl.loop(0, blocks)
     def _(b):
@@ -425,8 +407,7 @@
 
         @pl.when(b == 4)
         def _():
-            for e in range(1, RING):
-                weights_on(e).wait_recv()
+            arrived(wc_ref.at[:, pl.ds(0, RING - 1)], y_r.at[0])
 
         @pl.when((b >= 5) & (lax.rem(b, 2) == 1))
         def _():
@@ -436,48 +417,35 @@
         finish(g)
 
     def sums(d):
-        return send(ss_ref.at[tp], ss_ref.at[tp], (s_s.at[d - 1], s_r.at[d - 1]), at_tp(other_tp(d)))
+        return send(ss_ref.at[tp], ss_ref.at[tp], (s_s.at[0], s_r.at[0]), at_tp(other_tp(d)))
 
     for d in range(1, tp_n):
         sums(d).start()
 
     for j in range(xs):
-        for e in range(1, tp_n) if j == 0 else beside:
-            tokens_to(e, j).wait_send()
-        if j:
-            for way in range(2):
-                tokens_on(j, way).wait_send()
-    for d in range(1, tp_n):
-        weights_to(d).wait_send()
-    for e in range(1, RING):
-        weights_on(e).wait_send()
-    for d in range(1, kv_n):
-
-        @pl.when(serves(d))
-        def _(d=d):
-            give(d).wait_send()
+        arrived(tk_ref.at[pl.ds(0, len(beside) if j else tp_n - 1), 0], t_s.at[j])
+    arrived(tk_ref.at[pl.ds(0, 2), pl.ds(0, xs - 1)], tf_s.at[0])
+    arrived(chs_ref, ch_s.at[0])
+    arrived(wc_ref.at[pl.ds(0, tp_n - 1), 0], w_s.at[0])
+    arrived(wc_ref.at[:, pl.ds(0, RING - 1)], y_s.at[0])
+    for n in range(1, kv_n):
+
+        @pl.when(kv == kv_n - 1 - n)
+        def _(n=n):
+            arrived(out_ref.at[pl.ds(0, n)], b_s.at[0])
 
     for g in range(count):
 
         def drain(g=g):
-            for i in range(3):
-                spread(g, i).wait_send()
-            for i in range(2):
-                pass_on(g, i).wait_send()
-            for i in range(4):
-                relay(g, i).wait_send()
+            arrived(kvp_ref.at[pl.ds(0, 7), pl.ds(*groups[g])], k_s.at[g])
 
         when_group(g, drain)
 
-    @pl.loop(0, blocks)
-    def _(b):
-        for i in range(3):
-            heads_to(b, i).wait_send()
-
-    for g in range(pairs):
-        swap(g).wait()
-    for d in range(1, tp_n):
-        sums(d).wait()
+    arrived(ho_ref.at[pl.ds(0, xs - 1)], h_s.at[0])
+    arrived(px_ref, p_s.at[0])
+    arrived(ss_ref.at[pl.ds(0, tp_n - 1)], s_s.at[0])
+    arrived(px_ref, p_r.at[0])
+    arrived(ss_ref.at[pl.ds(0, tp_n - 1)], s_r.at[0])
     gains = ogain_ref[:, pl.ds(pl.multiple_of(tp * cols, cols), cols)]
     inverse = []
     for c in range(2):
@@ -488,7 +456,7 @@
 
     def store(g):
         part = pl.ds(2 * g * BLOCK, 2 * BLOCK)
-        return pltpu.make_async_copy(o_ref.at[part], out_hbm.at[part], oc.at[g])
+        return pltpu.make_async_copy(o_ref.at[part], out_hbm.at[part], oc.at[0])
 
     for g in range(pairs):
         for c in range(2):
@@ -498,8 +466,7 @@
             for u in range(2):
                 o_ref[pl.ds((2 * g + u) * BLOCK + c * half, half), :] = rows[u * half : (u + 1) * half]
         store(g).start()
-    for g in range(pairs):
-        store(g).wait()
+    arrived(o_ref, oc.at[0])
 
 
 def on_device(
@@ -528,9 +495,10 @@
     bf, f32, i32 = jnp.bfloat16, jnp.float32, jnp.int32
     dma = pltpu.SemaphoreType.DMA
     vmem = pl.BlockSpec(memory_space=pltpu.VMEM)
+    near = len(owner_groups(kv_n))
     sems = [
-        (xs, tp_n - 1), (xs, 2), (2,), (kv_n - 1,), (kv_n - 1,), (count, 3), (count, 2), (count, 4),
-        (tp_n - 1,), (RING - 1,), (blocks, 3), (blocks // 2,), (tp_n - 1,),
+        1, xs, 1, xs, xs, 2, 2, 1, 1, 1, near, count, count, count, count,
+        1, 1, 1, 1, 1, blocks // 2, 1, 1, 1, 1,
     ]
     return pl.pallas_call(
         functools.partial(kernel, kv_n, tp_n),
@@ -559,7 +527,7 @@
             pltpu.VMEM((blocks // 2, 2, BLOCK, cols), f32),
             pltpu.VMEM((blocks // 2, BLOCK, cols), f32),
             pltpu.VMEM((tp_n, blocks // 2, BLOCK), f32),
-            dma((2,)), dma((blocks // 2,)), *[dma(shape) for shape in sems for _ in range(2)],
+            dma((2,)), *[dma((n,)) for n in sems],
         ],
         compiler_params=pltpu.CompilerParams(
             collective_id=0, has_side_effects=True, vmem_limit_bytes=60 << 20

time: 65.5 us -> 62.4 us (0.953)
  Pallas kernels: 63.7 us -> 60.6 us
    pallas_call x1, Pallas kernels: 63.7 us -> 60.6 us  [on_device(): pl.pallas_call(functools.partial(kernel, kv_n, tp_n), out_shape=jax.Shape...]
where the time goes in v5:
time: 62.4 us; the launch traced here: 62.3 us
  Pallas kernels  60.6 us (97%)
  local copies, waits for them, and re-layouts  1.67 us (3%)
    pallas_call x1, Pallas kernels, on_device(): pl.pallas_call(functools.partial(kernel, kv_n, tp_n), out_shape=jax.Shape...  60.6 us
    unnamed x1, local copies, waits for them, and re-layouts  1.67 us

profile of v5, /device:TPU:201, one launch (start us, length us, event | category | flops | bytes accessed | tf_op | source)
XLA Modules:
  0.0 62.3 jit_solution(11841084411591956579)
XLA Ops:
  0.0 60.6 %shard_map.91 = bf16[1024,128]{1,0:T(8,128)(2,1)} custom-call(bf16[8,2,4,16,128]{4,3,2,1,0:T(8,128)(2,1)} %bitcast.5, bf16[1024,256]{1,0:T(8,128)(2,1)} %wq_ref.1, bf16[1024,128]{1,0:T(8,128)(2,1)} %wl_ref.1, f32[1,128]{1,0:T(1,128)} %bitcast.8, f32[1,128]{1,0:T(1,128)} %bitcast.9, bf16[2,64,128]{2,1,0:T(8,128)(2,1)} %bitcast.6, bf16[128,1024]{1,0:T(8,128)(2,1)} %w_ref.1, ...), custom_call_target="tpu_custom_call" | custom-call | tf_op jit(solution)/shard_map/pallas_call | solution.py:503
  60.6 1.7 %copy.11 = bf16[1024,128]{1,0:T(8,128)(2,1)} copy(bf16[1024,128]{1,0:T(8,128)(2,1)} %shard_map.91) | data formatting | bytes 524288

commit v6 on v5

--- a/solution.py
+++ b/solution.py
@@ -49,12 +49,13 @@
 
 def kernel(
     kv_n, tp_n,
-    tok_ref, wq_ref, wl_ref, qgain_ref, kgain_ref, vu_ref, w_ref, ogain_ref, chosen_ref, chosen_s,
-    out_hbm,
-    o_ref, tk_ref, wqs_ref, vus_ref, q_ref, lat_ref, out_ref, kvp_ref, kn_ref, vt_ref, bd_ref,
+    tok_in, wq_in, wl_in, qgain_in, kgain_in, vu_in, w_in, ogain_in, chosen_in,
+    o_ref,
+    chosen_ref, chosen_s, tok_ref, wl_ref, wq_ref, vu_ref, w_ref, qgain_ref, kgain_ref, ogain_ref,
+    tk_ref, wqs_ref, vus_ref, q_ref, lat_ref, out_ref, kvp_ref, kn_ref, vt_ref, bd_ref,
     map_ref, req_ref, chs_ref, map_s, chs_s,
     ho_ref, wc_ref, proj_ref, px_ref, ss_ref,
-    lc, oc, t_s, tf_s, t_r, tf_r, c_s, c_r, ch_s, ch_r, b_s, b_r, k_s, k_r, kf_r, kr_r,
+    in_s, lc, t_s, tf_s, t_r, tf_r, c_s, c_r, ch_s, ch_r, b_s, b_r, k_s, k_r, kf_r, kr_r,
     w_s, w_r, y_s, y_r, h_s, h_r, p_s, p_r, s_s, s_r,
 ):
     kv, tp = lax.axis_index("kv"), lax.axis_index("tp")
@@ -88,6 +89,16 @@
     for d in range(1, tp_n):
         pl.semaphore_signal(barrier, inc=1, device_id=at_tp(other_tp(d)), device_id_type=MESH)
 
+    loads = [
+        pltpu.make_async_copy(a, b, in_s.at[i])
+        for i, (a, b) in enumerate([
+            (chosen_in, chosen_ref), (chosen_in, chosen_s), (tok_in, tok_ref), (wl_in, wl_ref), (wq_in, wq_ref),
+            (vu_in, vu_ref), (w_in, w_ref), (qgain_in, qgain_ref), (kgain_in, kgain_ref), (ogain_in, ogain_ref),
+        ])
+    ]
+    for load in loads:
+        load.start()
+    loads[0].wait()
     lane = lax.broadcasted_iota(jnp.int32, (blocks, LANES), 1)
     halves = map_ref.shape[0]
     table = chosen_ref[...]
@@ -107,6 +118,8 @@
         req_ref[g] = prefix_in_owner(code, lane, blocks, True)[0:1]
 
     pltpu.make_async_copy(map_ref, map_s, lc.at[0]).start()
+    for load in loads[1:]:
+        load.wait()
     pl.semaphore_wait(barrier, kv_n - 1 + tp_n - 1)
 
     def chip(i):
@@ -160,7 +173,10 @@
     for e in range(1, tp_n):
         tokens_to(e, 0).start()
     for d in range(1, kv_n):
-        ask(d).start()
+
+        @pl.when(kv - d >= 0)
+        def _(d=d):
+            ask(d).start()
 
     for j in range(1, xs):
         for e in beside:
@@ -192,7 +208,12 @@
         if j < xs - 1:
             tokens_on(j + 1, 1).start()
 
-    arrived(chs_ref, ch_r.at[0])
+    for n in range(1, kv_n):
+
+        @pl.when(kv == kv_n - 1 - n)
+        def _(n=n):
+            arrived(chs_ref.at[pl.ds(0, n)], ch_r.at[0])
+
     to_smem = pltpu.make_async_copy(chs_ref, chs_s, lc.at[1])
     to_smem.start()
     arrived(tk_ref.at[pl.ds(0, tp_n - 1), 0], t_r.at[0])
@@ -227,6 +248,9 @@
         (blocks + (a - 1) * PER_OWNER, (b - a) * PER_OWNER) for a, b in remote
     ]
 
+    def direct(g):
+        return g == len(groups) - 1
+
     def halves_of(g):
         first, size = groups[g]
         cut = (size + 1) // 2
@@ -234,7 +258,7 @@
 
     def spread(g, i):
         part = kvp_ref.at[tp, pl.ds(*groups[g])]
-        where = sib if i == 2 else same_core(1 - 2 * i)
+        where = sib if i == 2 else same_core((1, -1, 0, 2)[i])
         return send(part, part, (k_s.at[g], (kr_r if i == 2 else k_r).at[g]), at_tp(where))
 
     def pass_on(g, way):
@@ -243,8 +267,8 @@
         return send(part, part, (k_s.at[g], kf_r.at[g]), at_tp(same_core(step)))
 
     def relay(g, i):
-        if i < 2:
-            part = kvp_ref.at[same_core(2 * i - 1), pl.ds(*groups[g])]
+        if i < 2 or direct(g):
+            part = kvp_ref.at[same_core((-1, 1, 2)[i]), pl.ds(*groups[g])]
         else:
             part = kvp_ref.at[same_core(2), halves_of(g)[i - 2]]
         return send(part, part, (k_s.at[g], kr_r.at[g]), at_tp(sib))
@@ -265,16 +289,17 @@
                     def _(n=n):
                         arrived(kvp_ref.at[tp, pl.ds(groups[g][0], n * PER_OWNER)], b_r.at[g - 1])
 
-            for i in range(3):
+            for i in range(3 + direct(g)):
                 spread(g, i).start()
 
         when_group(g, body)
 
     def pass_group(g):
         def body():
-            arrived(kvp_ref.at[pl.ds(0, 2), pl.ds(*groups[g])], k_r.at[g])
-            for i in range(2):
-                pass_on(g, i).start()
+            arrived(kvp_ref.at[pl.ds(0, 2 + direct(g)), pl.ds(*groups[g])], k_r.at[g])
+            for i in range(2 + direct(g)):
+                if not direct(g):
+                    pass_on(g, i).start()
                 relay(g, i).start()
 
         when_group(g, body)
@@ -331,21 +356,38 @@
     project(0)
     for j in range(1, xs):
         hand_tokens(j)
-    for step in range(1, count + 3):
+    def weights_step():
+        arrived(wc_ref.at[pl.ds(0, tp_n - 1), 0], w_r.at[0])
+        for e in range(1, RING):
+            weights_on(e).start()
+
+    normed = 0
+    projected = 1
+    for step in range(1, count + 1):
         if step < count:
             spread_group(step)
-        if step <= count:
+        if step < count or count == 1:
             pass_group(step - 1)
-        if 2 <= step <= count + 1:
+        if 2 <= step:
             relay_group(step - 2)
-        if 2 <= step <= xs:
-            project(step - 1)
-        if step >= 3:
-            norm_group(step - 3)
+        if step >= 2 and projected < xs and step < count:
+            project(projected)
+            projected += 1
         if step == 3:
-            arrived(wc_ref.at[pl.ds(0, tp_n - 1), 0], w_r.at[0])
-            for e in range(1, RING):
-                weights_on(e).start()
+            weights_step()
+        if step >= 4:
+            norm_group(normed)
+            normed += 1
+    for j in range(projected, xs):
+        project(j)
+    if count < 4:
+        weights_step()
+    for g in range(normed, max(count - 2, 0)):
+        norm_group(g)
+    if count > 1:
+        pass_group(count - 1)
+    for g in range(max(normed, count - 2), count):
+        norm_group(g)
 
     def listed(b, c):
         block = chosen_s[b, c]
@@ -425,7 +467,12 @@
     for j in range(xs):
         arrived(tk_ref.at[pl.ds(0, len(beside) if j else tp_n - 1), 0], t_s.at[j])
     arrived(tk_ref.at[pl.ds(0, 2), pl.ds(0, xs - 1)], tf_s.at[0])
-    arrived(chs_ref, ch_s.at[0])
+    for n in range(1, kv_n):
+
+        @pl.when(kv == n)
+        def _(n=n):
+            arrived(chs_ref.at[pl.ds(0, n)], ch_s.at[0])
+
     arrived(wc_ref.at[pl.ds(0, tp_n - 1), 0], w_s.at[0])
     arrived(wc_ref.at[:, pl.ds(0, RING - 1)], y_s.at[0])
     for n in range(1, kv_n):
@@ -454,10 +501,6 @@
             total = total + ss_ref[2 * p + c]
         inverse.append(lax.rsqrt(total / (cols * tp_n) + epsilon))
 
-    def store(g):
-        part = pl.ds(2 * g * BLOCK, 2 * BLOCK)
-        return pltpu.make_async_copy(o_ref.at[part], out_hbm.at[part], oc.at[0])
-
     for g in range(pairs):
         for c in range(2):
             scale = jnp.broadcast_to(inverse[c][g : g + 1], (BLOCK, BLOCK)).T
@@ -465,8 +508,6 @@
             rows = (proj_ref[g, c] * scale * gains).astype(jnp.bfloat16)
             for u in range(2):
                 o_ref[pl.ds((2 * g + u) * BLOCK + c * half, half), :] = rows[u * half : (u + 1) * half]
-        store(g).start()
-    arrived(o_ref, oc.at[0])
 
 
 def on_device(
@@ -497,16 +538,25 @@
     vmem = pl.BlockSpec(memory_space=pltpu.VMEM)
     near = len(owner_groups(kv_n))
     sems = [
-        1, xs, 1, xs, xs, 2, 2, 1, 1, 1, near, count, count, count, count,
+        xs, 1, xs, xs, 2, 2, 1, 1, 1, near, count, count, count, count,
         1, 1, 1, 1, 1, blocks // 2, 1, 1, 1, 1,
     ]
     return pl.pallas_call(
         functools.partial(kernel, kv_n, tp_n),
         out_shape=jax.ShapeDtypeStruct((toks, cols), bf),
-        in_specs=[vmem] * 9 + [pl.BlockSpec(memory_space=pltpu.SMEM)],
-        out_specs=pl.BlockSpec(memory_space=pl.ANY),
+        in_specs=[pl.BlockSpec(memory_space=pltpu.HBM)] * 9,
+        out_specs=vmem,
         scratch_shapes=[
-            pltpu.VMEM((toks, cols), bf),
+            pltpu.VMEM(chosen.shape, i32),
+            pltpu.SMEM(chosen.shape, i32),
+            pltpu.VMEM((blocks, 2, xs, piece, feat), bf),
+            pltpu.VMEM(latent_weight.shape, bf),
+            pltpu.VMEM(query_weight.shape, bf),
+            pltpu.VMEM((value_up.shape[0], value_up.shape[2], value_up.shape[1]), bf),
+            pltpu.VMEM(out_weight.shape, bf),
+            pltpu.VMEM((1, width), f32),
+            pltpu.VMEM((1, width), f32),
+            pltpu.VMEM((1, cols * tp_n), f32),
             pltpu.VMEM((tp_n, xs, blocks, piece, feat), bf),
             pltpu.VMEM(query_weight.shape, bf),
             pltpu.VMEM((value_up.shape[0], value_up.shape[2], value_up.shape[1]), bf),
@@ -527,15 +577,18 @@
             pltpu.VMEM((blocks // 2, 2, BLOCK, cols), f32),
             pltpu.VMEM((blocks // 2, BLOCK, cols), f32),
             pltpu.VMEM((tp_n, blocks // 2, BLOCK), f32),
-            dma((2,)), *[dma((n,)) for n in sems],
+            dma((10,)), dma((2,)), *[dma((n,)) for n in sems],
         ],
         compiler_params=pltpu.CompilerParams(
-            collective_id=0, has_side_effects=True, vmem_limit_bytes=60 << 20
+            collective_id=0, has_side_effects=True, vmem_limit_bytes=24 << 20
         ),
-    )(
-        tokens.reshape(blocks, 2, xs, piece, feat), query_weight, latent_weight, query_gain[None, :],
-        key_gain[None, :], jnp.swapaxes(value_up, 1, 2), out_weight, out_gain[None, :], chosen, chosen,
-    )
+    )(*[
+        pltpu.with_memory_space_constraint(a, pltpu.HBM)
+        for a in (
+            tokens.reshape(blocks, 2, xs, piece, feat), query_weight, latent_weight, query_gain[None, :],
+            key_gain[None, :], jnp.swapaxes(value_up, 1, 2), out_weight, out_gain[None, :], chosen,
+        )
+    ])
 
 
 def solution(mesh):

time: 62.4 us -> 58.3 us (0.934)
  Pallas kernels: 60.6 us -> 57.5 us
  local copies, waits for them, and re-layouts: 1.67 us -> 0.71 us
    pallas_call x1, Pallas kernels: 60.6 us -> 57.5 us  [on_device(): pl.pallas_call(functools.partial(kernel, kv_n, tp_n), out_shape=jax.Shape...]
    unnamed x1, local copies, waits for them, and re-layouts: 1.67 us -> 0.71 us
where the time goes in v6:
time: 58.3 us; the launch traced here: 58.2 us
  Pallas kernels  57.5 us (99%)
  local copies, waits for them, and re-layouts  0.71 us (1%)
    pallas_call x1, Pallas kernels, on_device(): pl.pallas_call(functools.partial(kernel, kv_n, tp_n), out_shape=jax.Shape...  57.5 us

profile of v6, /device:TPU:201, one launch (start us, length us, event | category | flops | bytes accessed | tf_op | source)
XLA Modules:
  0.0 58.2 jit_solution(7274160350453803384)
XLA Ops:
  0.0 57.5 %shard_map.91 = bf16[1024,128]{1,0:T(8,128)(2,1)S(1)} custom-call(bf16[8,2,4,16,128]{4,3,2,1,0:T(8,128)(2,1)} %bitcast.5, bf16[1024,256]{1,0:T(8,128)(2,1)} %wq_in.1, bf16[1024,128]{1,0:T(8,128)(2,1)} %wl_in.1, f32[1,128]{1,0:T(1,128)} %bitcast.8, f32[1,128]{1,0:T(1,128)} %bitcast.9, bf16[2,64,128]{2,1,0:T(8,128)(2,1)} %bitcast.6, bf16[128,1024]{1,0:T(8,128)(2,1)} %w_in.1, ...), custom_call_target="tpu_custom_call" | custom-call | tf_op jit(solution)/shard_map/pallas_call | solution.py:544
  57.5 0.7 %copy.11 = bf16[1024,128]{1,0:T(8,128)(2,1)} copy(bf16[1024,128]{1,0:T(8,128)(2,1)S(1)} %shard_map.91) | data formatting | bytes 524288

commit v7 on v6

--- a/solution.py
+++ b/solution.py
@@ -44,7 +44,8 @@
 
 
 def owner_groups(kv_n):
-    return [(d, min(d + OWNERS, kv_n)) for d in range(1, kv_n, OWNERS)]
+    spans = [(d, min(d + OWNERS, kv_n)) for d in range(1, kv_n, OWNERS)]
+    return spans[:1] + spans[:1:-1] + spans[1:2]
 
 
 def kernel(
@@ -170,7 +171,7 @@
         send(vu_ref, vus_ref, (c_s.at[1], c_r.at[1]), at_tp(sib)),
     ]
 
-    for e in range(1, tp_n):
+    for e in (4, 5, 2, 3, 6, 7, 1):
         tokens_to(e, 0).start()
     for d in range(1, kv_n):
 
@@ -183,9 +184,6 @@
             tokens_to(e, j).start()
     for copy in to_sib:
         copy.start()
-    for d in range(1, tp_n):
-        weights_to(d).start()
-
     for p in range(xs):
         tk_ref[tp, p] = tok_ref[:, core, p]
     wc_ref[tp, y] = w_ref[
@@ -228,9 +226,14 @@
     def slots_of(d):
         return pl.ds(blocks + (d - 1) * PER_OWNER, PER_OWNER)
 
+    remote = owner_groups(kv_n)
+
+    def span_of(d):
+        return next(i for i, (a, b) in enumerate(remote) if a <= d < b)
+
     def give(d):
         return send(
-            out_ref.at[d - 1], kvp_ref.at[tp, slots_of(d)], (b_s.at[0], b_r.at[(d - 1) // OWNERS]), at_kv(lax.rem(kv + d, kv_n))
+            out_ref.at[d - 1], kvp_ref.at[tp, slots_of(d)], (b_s.at[0], b_r.at[span_of(d)]), at_kv(lax.rem(kv + d, kv_n))
         )
 
     at_lane = lax.rem(kv, per_row) * blocks + blocks - 1
@@ -243,7 +246,6 @@
                 out_ref[d - 1, k] = lat_ref[(code >> (3 * k)) & (blocks - 1)]
             give(d).start()
 
-    remote = owner_groups(kv_n)
     groups = [(0, blocks)] + [
         (blocks + (a - 1) * PER_OWNER, (b - a) * PER_OWNER) for a, b in remote
     ]
@@ -370,20 +372,20 @@
             pass_group(step - 1)
         if 2 <= step:
             relay_group(step - 2)
+        if step == min(2, count):
+            for d in range(1, tp_n):
+                weights_to(d).start()
         if step >= 2 and projected < xs and step < count:
             project(projected)
             projected += 1
-        if step == 3:
-            weights_step()
         if step >= 4:
             norm_group(normed)
             normed += 1
     for j in range(projected, xs):
         project(j)
-    if count < 4:
-        weights_step()
     for g in range(normed, max(count - 2, 0)):
         norm_group(g)
+    weights_step()
     if count > 1:
         pass_group(count - 1)
     for g in range(max(normed, count - 2), count):
@@ -447,15 +449,8 @@
         for i in range(3):
             heads_to(b, i).start()
 
-        @pl.when(b == 4)
-        def _():
-            arrived(wc_ref.at[:, pl.ds(0, RING - 1)], y_r.at[0])
-
-        @pl.when((b >= 5) & (lax.rem(b, 2) == 1))
-        def _():
-            finish((b - 5) // 2)
-
-    for g in range(max(pairs - 2, 0), pairs):
+    arrived(wc_ref.at[:, pl.ds(0, RING - 1)], y_r.at[0])
+    for g in range(pairs):
         finish(g)
 
     def sums(d):

time: 58.3 us -> 56.8 us (0.974); the launches traced: 58.2 us -> 55.9 us
  Pallas kernels: 57.5 us -> 55.2 us
    pallas_call x1, Pallas kernels: 57.5 us -> 55.2 us  [on_device(): pl.pallas_call(functools.partial(kernel, kv_n, tp_n), out_shape=jax.Shape...]
where the time goes in v7:
time: 56.8 us; the launch traced here: 55.9 us
  Pallas kernels  55.2 us (97%)
  local copies, waits for them, and re-layouts  0.71 us (1%)
    pallas_call x1, Pallas kernels, on_device(): pl.pallas_call(functools.partial(kernel, kv_n, tp_n), out_shape=jax.Shape...  55.2 us

profile of v7, /device:TPU:201, one launch (start us, length us, event | category | flops | bytes accessed | tf_op | source)
XLA Modules:
  0.0 55.9 jit_solution(8997874887263045229)
XLA Ops:
  0.0 55.2 %shard_map.91 = bf16[1024,128]{1,0:T(8,128)(2,1)S(1)} custom-call(bf16[8,2,4,16,128]{4,3,2,1,0:T(8,128)(2,1)} %bitcast.5, bf16[1024,256]{1,0:T(8,128)(2,1)} %wq_in.1, bf16[1024,128]{1,0:T(8,128)(2,1)} %wl_in.1, f32[1,128]{1,0:T(1,128)} %bitcast.8, f32[1,128]{1,0:T(1,128)} %bitcast.9, bf16[2,64,128]{2,1,0:T(8,128)(2,1)} %bitcast.6, bf16[128,1024]{1,0:T(8,128)(2,1)} %w_in.1, ...), custom_call_target="tpu_custom_call" | custom-call | tf_op jit(solution)/shard_map/pallas_call | solution.py:539
  55.2 0.7 %copy.11 = bf16[1024,128]{1,0:T(8,128)(2,1)} copy(bf16[1024,128]{1,0:T(8,128)(2,1)S(1)} %shard_map.91) | data formatting | bytes 524288

commit v8 on v7

--- a/solution.py
+++ b/solution.py
@@ -251,7 +251,7 @@
     ]
 
     def direct(g):
-        return g == len(groups) - 1
+        return g >= min(1, len(groups) - 1)
 
     def halves_of(g):
         first, size = groups[g]
@@ -308,9 +308,10 @@
 
     def relay_group(g):
         def body():
-            arrived(kvp_ref.at[0, pl.ds(*groups[g])], kf_r.at[g])
-            for i in range(2):
-                relay(g, i + 2).start()
+            if not direct(g):
+                arrived(kvp_ref.at[0, pl.ds(*groups[g])], kf_r.at[g])
+                for i in range(2):
+                    relay(g, i + 2).start()
 
         when_group(g, body)
 
@@ -363,32 +364,28 @@
         for e in range(1, RING):
             weights_on(e).start()
 
-    normed = 0
-    projected = 1
-    for step in range(1, count + 1):
-        if step < count:
-            spread_group(step)
-        if step < count or count == 1:
-            pass_group(step - 1)
-        if 2 <= step:
-            relay_group(step - 2)
-        if step == min(2, count):
-            for d in range(1, tp_n):
-                weights_to(d).start()
-        if step >= 2 and projected < xs and step < count:
-            project(projected)
-            projected += 1
-        if step >= 4:
+    for g in range(1, count):
+        spread_group(g)
+        if g <= 2:
+            pass_group(g - 1)
+    if count < 3:
+        pass_group(count - 1)
+    for d in range(1, tp_n):
+        weights_to(d).start()
+    if not direct(0):
+        relay_group(0)
+    passed, normed = min(count, 2), 0
+    for j in range(1, xs):
+        project(j)
+    norm_group(normed)
+    normed += 1
+    for g in range(passed, count):
+        pass_group(g)
+        if normed < g:
             norm_group(normed)
             normed += 1
-    for j in range(projected, xs):
-        project(j)
-    for g in range(normed, max(count - 2, 0)):
-        norm_group(g)
     weights_step()
-    if count > 1:
-        pass_group(count - 1)
-    for g in range(max(normed, count - 2), count):
+    for g in range(normed, count):
         norm_group(g)
 
     def listed(b, c):

time: 56.8 us -> 55.1 us (0.970)
  Pallas kernels: 55.2 us -> 53.5 us
    pallas_call x1, Pallas kernels: 55.2 us -> 53.5 us  [on_device(): pl.pallas_call(functools.partial(kernel, kv_n, tp_n), out_shape=jax.Shape...]
where the time goes in v8:
time: 55.1 us; the launch traced here: 54.2 us
  Pallas kernels  53.5 us (97%)
  local copies, waits for them, and re-layouts  0.71 us (1%)
    pallas_call x1, Pallas kernels, on_device(): pl.pallas_call(functools.partial(kernel, kv_n, tp_n), out_shape=jax.Shape...  53.5 us

profile of v8, /device:TPU:201, one launch (start us, length us, event | category | flops | bytes accessed | tf_op | source)
XLA Modules:
  0.0 54.2 jit_solution(3854181390003704437)
XLA Ops:
  0.0 53.5 %shard_map.91 = bf16[1024,128]{1,0:T(8,128)(2,1)S(1)} custom-call(bf16[8,2,4,16,128]{4,3,2,1,0:T(8,128)(2,1)} %bitcast.5, bf16[1024,256]{1,0:T(8,128)(2,1)} %wq_in.1, bf16[1024,128]{1,0:T(8,128)(2,1)} %wl_in.1, f32[1,128]{1,0:T(1,128)} %bitcast.8, f32[1,128]{1,0:T(1,128)} %bitcast.9, bf16[2,64,128]{2,1,0:T(8,128)(2,1)} %bitcast.6, bf16[128,1024]{1,0:T(8,128)(2,1)} %w_in.1, ...), custom_call_target="tpu_custom_call" | custom-call | tf_op jit(solution)/shard_map/pallas_call | solution.py:536
  53.5 0.7 %copy.11 = bf16[1024,128]{1,0:T(8,128)(2,1)} copy(bf16[1024,128]{1,0:T(8,128)(2,1)S(1)} %shard_map.91) | data formatting | bytes 524288

commit v9 on v8

--- a/solution.py
+++ b/solution.py
@@ -44,8 +44,11 @@
 
 
 def owner_groups(kv_n):
-    spans = [(d, min(d + OWNERS, kv_n)) for d in range(1, kv_n, OWNERS)]
-    return spans[:1] + spans[:1:-1] + spans[1:2]
+    rising = [(d, min(d + OWNERS, kv_n)) for d in range(1, kv_n, OWNERS)]
+    top = kv_n - RING
+    if top <= 3 * OWNERS:
+        return rising, rising
+    return rising, [(1, 1 + OWNERS), (top - OWNERS, top), (1 + OWNERS, top - OWNERS)]
 
 
 def kernel(
@@ -226,10 +229,11 @@
     def slots_of(d):
         return pl.ds(blocks + (d - 1) * PER_OWNER, PER_OWNER)
 
-    remote = owner_groups(kv_n)
+    rising, split = owner_groups(kv_n)
 
     def span_of(d):
-        return next(i for i, (a, b) in enumerate(remote) if a <= d < b)
+        index = [next((i for i, (a, b) in enumerate(spans) if a <= d < b), 0) for spans in (rising, split)]
+        return jnp.where(kv + d >= kv_n - RING, index[0], index[1])
 
     def give(d):
         return send(
@@ -246,96 +250,7 @@
                 out_ref[d - 1, k] = lat_ref[(code >> (3 * k)) & (blocks - 1)]
             give(d).start()
 
-    groups = [(0, blocks)] + [
-        (blocks + (a - 1) * PER_OWNER, (b - a) * PER_OWNER) for a, b in remote
-    ]
-
-    def direct(g):
-        return g >= min(1, len(groups) - 1)
-
-    def halves_of(g):
-        first, size = groups[g]
-        cut = (size + 1) // 2
-        return [pl.ds(first, cut), pl.ds(first + cut, size - cut)]
-
-    def spread(g, i):
-        part = kvp_ref.at[tp, pl.ds(*groups[g])]
-        where = sib if i == 2 else same_core((1, -1, 0, 2)[i])
-        return send(part, part, (k_s.at[g], (kr_r if i == 2 else k_r).at[g]), at_tp(where))
-
-    def pass_on(g, way):
-        step = 1 - 2 * way
-        part = kvp_ref.at[same_core(-step), halves_of(g)[way]]
-        return send(part, part, (k_s.at[g], kf_r.at[g]), at_tp(same_core(step)))
-
-    def relay(g, i):
-        if i < 2 or direct(g):
-            part = kvp_ref.at[same_core((-1, 1, 2)[i]), pl.ds(*groups[g])]
-        else:
-            part = kvp_ref.at[same_core(2), halves_of(g)[i - 2]]
-        return send(part, part, (k_s.at[g], kr_r.at[g]), at_tp(sib))
-
-    def when_group(g, body):
-        if g == 0:
-            body()
-        else:
-            pl.when(kv >= remote[g - 1][0])(body)
-
-    def spread_group(g):
-        def body():
-            if g:
-                a, b = remote[g - 1]
-                for n in range(1, b - a + 1):
-
-                    @pl.when((kv >= b - 1) if n == b - a else (kv == a + n - 1))
-                    def _(n=n):
-                        arrived(kvp_ref.at[tp, pl.ds(groups[g][0], n * PER_OWNER)], b_r.at[g - 1])
-
-            for i in range(3 + direct(g)):
-                spread(g, i).start()
-
-        when_group(g, body)
-
-    def pass_group(g):
-        def body():
-            arrived(kvp_ref.at[pl.ds(0, 2 + direct(g)), pl.ds(*groups[g])], k_r.at[g])
-            for i in range(2 + direct(g)):
-                if not direct(g):
-                    pass_on(g, i).start()
-                relay(g, i).start()
-
-        when_group(g, body)
-
-    def relay_group(g):
-        def body():
-            if not direct(g):
-                arrived(kvp_ref.at[0, pl.ds(*groups[g])], kf_r.at[g])
-                for i in range(2):
-                    relay(g, i + 2).start()
-
-        when_group(g, body)
-
     gain_k = kgain_ref[...]
-
-    def norm_group(g):
-        def body():
-            arrived(kvp_ref.at[pl.ds(0, 4), pl.ds(*groups[g])], kr_r.at[g])
-
-            first, size = groups[g]
-            each = next(n for n in (4, 2, 1) if size % n == 0)
-
-            @pl.loop(0, size // each)
-            def _(i):
-                for u in range(each):
-                    slot = first + i * each + u
-                    rows = jnp.concatenate(
-                        [kvp_ref[p * 2 + c, slot] for c in range(2) for p in range(xs)], axis=0
-                    )
-                    kn_ref[slot] = rms_scale(rows, gain_k)
-                    vt_ref[slot, 0:width, :] = rows.T
-
-        when_group(g, body)
-
     gain_q = qgain_ref[...] * (width**-0.5 * 1.4426950408889634)
 
     def project(j):
@@ -349,44 +264,142 @@
                 part = rms_scale(qs[:, h * width : (h + 1) * width], gain_q)
                 q_ref[at * heads + h, p] = part.reshape(blocks, piece, width)
 
-    spread_group(0)
-    for copy in to_sib:
-        copy.wait()
-    for v, at in ((vu_ref, core), (vus_ref, 1 - core)):
-        for h in range(heads):
-            bd_ref[at, h * vdim : (h + 1) * vdim, h * width : (h + 1) * width] = v[h]
-    count = len(groups)
-    project(0)
-    for j in range(1, xs):
-        hand_tokens(j)
-    def weights_step():
-        arrived(wc_ref.at[pl.ds(0, tp_n - 1), 0], w_r.at[0])
-        for e in range(1, RING):
-            weights_on(e).start()
-
-    for g in range(1, count):
-        spread_group(g)
-        if g <= 2:
-            pass_group(g - 1)
-    if count < 3:
-        pass_group(count - 1)
-    for d in range(1, tp_n):
-        weights_to(d).start()
-    if not direct(0):
-        relay_group(0)
-    passed, normed = min(count, 2), 0
-    for j in range(1, xs):
-        project(j)
-    norm_group(normed)
-    normed += 1
-    for g in range(passed, count):
-        pass_group(g)
-        if normed < g:
-            norm_group(normed)
-            normed += 1
-    weights_step()
-    for g in range(normed, count):
-        norm_group(g)
+    def exchange(remote):
+        groups = [(0, blocks)] + [
+            (blocks + (a - 1) * PER_OWNER, (b - a) * PER_OWNER) for a, b in remote
+        ]
+
+        def direct(g):
+            return g >= min(1, len(groups) - 1)
+
+        def halves_of(g):
+            first, size = groups[g]
+            cut = (size + 1) // 2
+            return [pl.ds(first, cut), pl.ds(first + cut, size - cut)]
+
+        def spread(g, i):
+            part = kvp_ref.at[tp, pl.ds(*groups[g])]
+            where = sib if i == 2 else same_core((1, -1, 0, 2)[i])
+            return send(part, part, (k_s.at[g], (kr_r if i == 2 else k_r).at[g]), at_tp(where))
+
+        def pass_on(g, way):
+            step = 1 - 2 * way
+            part = kvp_ref.at[same_core(-step), halves_of(g)[way]]
+            return send(part, part, (k_s.at[g], kf_r.at[g]), at_tp(same_core(step)))
+
+        def relay(g, i):
+            if i < 2 or direct(g):
+                part = kvp_ref.at[same_core((-1, 1, 2)[i]), pl.ds(*groups[g])]
+            else:
+                part = kvp_ref.at[same_core(2), halves_of(g)[i - 2]]
+            return send(part, part, (k_s.at[g], kr_r.at[g]), at_tp(sib))
+
+        def when_group(g, body):
+            if g == 0:
+                body()
+            else:
+                pl.when(kv >= remote[g - 1][0])(body)
+
+        def spread_group(g):
+            def body():
+                if g:
+                    a, b = remote[g - 1]
+                    for n in range(1, b - a + 1):
+
+                        @pl.when((kv >= b - 1) if n == b - a else (kv == a + n - 1))
+                        def _(n=n):
+                            arrived(kvp_ref.at[tp, pl.ds(groups[g][0], n * PER_OWNER)], b_r.at[g - 1])
+
+                for i in range(3 + direct(g)):
+                    spread(g, i).start()
+
+            when_group(g, body)
+
+        def pass_group(g):
+            def body():
+                arrived(kvp_ref.at[pl.ds(0, 2 + direct(g)), pl.ds(*groups[g])], k_r.at[g])
+                for i in range(2 + direct(g)):
+                    if not direct(g):
+                        pass_on(g, i).start()
+                    relay(g, i).start()
+
+            when_group(g, body)
+
+        def relay_group(g):
+            def body():
+                if not direct(g):
+                    arrived(kvp_ref.at[0, pl.ds(*groups[g])], kf_r.at[g])
+                    for i in range(2):
+                        relay(g, i + 2).start()
+
+            when_group(g, body)
+
+        def norm_group(g):
+            def body():
+                arrived(kvp_ref.at[pl.ds(0, 4), pl.ds(*groups[g])], kr_r.at[g])
+
+                first, size = groups[g]
+                each = next(n for n in (4, 2, 1) if size % n == 0)
+
+                @pl.loop(0, size // each)
+                def _(i):
+                    for u in range(each):
+                        slot = first + i * each + u
+                        rows = jnp.concatenate(
+                            [kvp_ref[p * 2 + c, slot] for c in range(2) for p in range(xs)], axis=0
+                        )
+                        kn_ref[slot] = rms_scale(rows, gain_k)
+                        vt_ref[slot, 0:width, :] = rows.T
+
+            when_group(g, body)
+
+        spread_group(0)
+        for copy in to_sib:
+            copy.wait()
+        for v, at in ((vu_ref, core), (vus_ref, 1 - core)):
+            for h in range(heads):
+                bd_ref[at, h * vdim : (h + 1) * vdim, h * width : (h + 1) * width] = v[h]
+        count = len(groups)
+        project(0)
+        for j in range(1, xs):
+            hand_tokens(j)
+        def weights_step():
+            arrived(wc_ref.at[pl.ds(0, tp_n - 1), 0], w_r.at[0])
+            for e in range(1, RING):
+                weights_on(e).start()
+
+        for g in range(1, count):
+            spread_group(g)
+            if g <= 2:
+                pass_group(g - 1)
+        if count < 3:
+            pass_group(count - 1)
+        for d in range(1, tp_n):
+            weights_to(d).start()
+        if not direct(0):
+            relay_group(0)
+        passed, normed = min(count, 2), 0
+        for j in range(1, xs):
+            project(j)
+        norm_group(normed)
+        normed += 1
+        for g in range(passed, count):
+            pass_group(g)
+            if normed < g:
+                norm_group(normed)
+                normed += 1
+        weights_step()
+        for g in range(normed, count):
+            norm_group(g)
+
+
+    @pl.when(kv >= kv_n - RING)
+    def _():
+        exchange(rising)
+
+    @pl.when(kv < kv_n - RING)
+    def _():
+        exchange(split)
 
     def listed(b, c):
         block = chosen_s[b, c]
@@ -473,12 +486,22 @@
         def _(n=n):
             arrived(out_ref.at[pl.ds(0, n)], b_s.at[0])
 
-    for g in range(count):
-
-        def drain(g=g):
-            arrived(kvp_ref.at[pl.ds(0, 7), pl.ds(*groups[g])], k_s.at[g])
-
-        when_group(g, drain)
+    def drain(remote):
+        arrived(kvp_ref.at[pl.ds(0, 7), pl.ds(0, blocks)], k_s.at[0])
+        for g, (a, b) in enumerate(remote):
+
+            @pl.when(kv >= a)
+            def _(g=g, a=a, b=b):
+                part = pl.ds(blocks + (a - 1) * PER_OWNER, (b - a) * PER_OWNER)
+                arrived(kvp_ref.at[pl.ds(0, 7), part], k_s.at[g + 1])
+
+    @pl.when(kv >= kv_n - RING)
+    def _():
+        drain(rising)
+
+    @pl.when(kv < kv_n - RING)
+    def _():
+        drain(split)
 
     arrived(ho_ref.at[pl.ds(0, xs - 1)], h_s.at[0])
     arrived(px_ref, p_s.at[0])
@@ -524,11 +547,11 @@
     piece = BLOCK // tp_n
     slots = blocks + (kv_n - 1) * PER_OWNER
     halves = max(1, kv_n * blocks // LANES)
-    count = 1 + len(owner_groups(kv_n))
+    count = 1 + len(owner_groups(kv_n)[0])
     bf, f32, i32 = jnp.bfloat16, jnp.float32, jnp.int32
     dma = pltpu.SemaphoreType.DMA
     vmem = pl.BlockSpec(memory_space=pltpu.VMEM)
-    near = len(owner_groups(kv_n))
+    near = len(owner_groups(kv_n)[0])
     sems = [
         xs, 1, xs, xs, 2, 2, 1, 1, 1, near, count, count, count, count,
         1, 1, 1, 1, 1, blocks // 2, 1, 1, 1, 1,

time: 55.1 us -> 54.3 us (0.985)
  no operation moved by 1% of the time
where the time goes in v9:
time: 54.3 us; the launch traced here: 53.7 us
  Pallas kernels  53 us (98%)
  local copies, waits for them, and re-layouts  0.71 us (1%)
    pallas_call x1, Pallas kernels, on_device(): pl.pallas_call(functools.partial(kernel, kv_n, tp_n), out_shape=jax.Shape...  53 us

profile of v9, /device:TPU:201, one launch (start us, length us, event | category | flops | bytes accessed | tf_op | source)
XLA Modules:
  0.0 53.7 jit_solution(8833080016768716720)
XLA Ops:
  0.0 53.0 %shard_map.91 = bf16[1024,128]{1,0:T(8,128)(2,1)S(1)} custom-call(bf16[8,2,4,16,128]{4,3,2,1,0:T(8,128)(2,1)} %bitcast.5, bf16[1024,256]{1,0:T(8,128)(2,1)} %wq_in.1, bf16[1024,128]{1,0:T(8,128)(2,1)} %wl_in.1, f32[1,128]{1,0:T(1,128)} %bitcast.8, f32[1,128]{1,0:T(1,128)} %bitcast.9, bf16[2,64,128]{2,1,0:T(8,128)(2,1)} %bitcast.6, bf16[128,1024]{1,0:T(8,128)(2,1)} %w_in.1, ...), custom_call_target="tpu_custom_call" | custom-call | tf_op jit(solution)/shard_map/pallas_call | solution.py:559
  53.0 0.7 %copy.11 = bf16[1024,128]{1,0:T(8,128)(2,1)} copy(bf16[1024,128]{1,0:T(8,128)(2,1)S(1)} %shard_map.91) | data formatting | bytes 524288

commit v10 on v9

--- a/solution.py
+++ b/solution.py
@@ -44,11 +44,16 @@
 
 
 def owner_groups(kv_n):
-    rising = [(d, min(d + OWNERS, kv_n)) for d in range(1, kv_n, OWNERS)]
-    top = kv_n - RING
-    if top <= 3 * OWNERS:
-        return rising, rising
-    return rising, [(1, 1 + OWNERS), (top - OWNERS, top), (1 + OWNERS, top - OWNERS)]
+    if kv_n != 8 * RING:
+        return [(0, kv_n, [(d, min(d + OWNERS, kv_n)) for d in range(1, kv_n, OWNERS)])]
+    return [
+        (0, 8, [(1, 8)]),
+        (8, 16, [(1, 7), (7, 12), (12, 16)]),
+        (16, 20, [(1, 9), (9, 15), (15, 20)]),
+        (20, 24, [(1, 9), (17, 24), (9, 13), (13, 17)]),
+        (24, 28, [(1, 9), (20, 28), (9, 15), (15, 20)]),
+        (28, 32, [(1, 9), (9, 17), (17, 25), (25, 32)]),
+    ]
 
 
 def kernel(
@@ -229,11 +234,14 @@
     def slots_of(d):
         return pl.ds(blocks + (d - 1) * PER_OWNER, PER_OWNER)
 
-    rising, split = owner_groups(kv_n)
+    plans = owner_groups(kv_n)
 
     def span_of(d):
-        index = [next((i for i, (a, b) in enumerate(spans) if a <= d < b), 0) for spans in (rising, split)]
-        return jnp.where(kv + d >= kv_n - RING, index[0], index[1])
+        index = 0
+        for low, _, spans in plans:
+            here = next((i for i, (a, b) in enumerate(spans) if a <= d < b), 0)
+            index = jnp.where(kv + d >= low, here, index)
+        return index
 
     def give(d):
         return send(
@@ -393,13 +401,11 @@
             norm_group(g)
 
 
-    @pl.when(kv >= kv_n - RING)
-    def _():
-        exchange(rising)
-
-    @pl.when(kv < kv_n - RING)
-    def _():
-        exchange(split)
+    for low, high, spans in plans:
+
+        @pl.when((kv >= low) & (kv < high))
+        def _(spans=spans):
+            exchange(spans)
 
     def listed(b, c):
         block = chosen_s[b, c]
@@ -495,13 +501,11 @@
                 part = pl.ds(blocks + (a - 1) * PER_OWNER, (b - a) * PER_OWNER)
                 arrived(kvp_ref.at[pl.ds(0, 7), part], k_s.at[g + 1])
 
-    @pl.when(kv >= kv_n - RING)
-    def _():
-        drain(rising)
-
-    @pl.when(kv < kv_n - RING)
-    def _():
-        drain(split)
+    for low, high, spans in plans:
+
+        @pl.when((kv >= low) & (kv < high))
+        def _(spans=spans):
+            drain(spans)
 
     arrived(ho_ref.at[pl.ds(0, xs - 1)], h_s.at[0])
     arrived(px_ref, p_s.at[0])
@@ -547,11 +551,11 @@
     piece = BLOCK // tp_n
     slots = blocks + (kv_n - 1) * PER_OWNER
     halves = max(1, kv_n * blocks // LANES)
-    count = 1 + len(owner_groups(kv_n)[0])
+    near = max(len(spans) for _, _, spans in owner_groups(kv_n))
+    count = near + 1
     bf, f32, i32 = jnp.bfloat16, jnp.float32, jnp.int32
     dma = pltpu.SemaphoreType.DMA
     vmem = pl.BlockSpec(memory_space=pltpu.VMEM)
-    near = len(owner_groups(kv_n)[0])
     sems = [
         xs, 1, xs, xs, 2, 2, 1, 1, 1, near, count, count, count, count,
         1, 1, 1, 1, 1, blocks // 2, 1, 1, 1, 1,

time: 54.3 us -> 53.4 us (0.983)
  Pallas kernels: 53 us -> 52 us
    pallas_call x1, Pallas kernels: 53 us -> 52 us  [on_device(): pl.pallas_call(functools.partial(kernel, kv_n, tp_n), out_shape=jax.Shape...]
where the time goes in v10:
time: 53.4 us; the launch traced here: 52.7 us
  Pallas kernels  52 us (97%)
  local copies, waits for them, and re-layouts  0.71 us (1%)
    pallas_call x1, Pallas kernels, on_device(): pl.pallas_call(functools.partial(kernel, kv_n, tp_n), out_shape=jax.Shape...  52 us

profile of v10, /device:TPU:201, one launch (start us, length us, event | category | flops | bytes accessed | tf_op | source)
XLA Modules:
  0.0 52.7 jit_solution(5056996894080610571)
XLA Ops:
  0.0 52.0 %shard_map.91 = bf16[1024,128]{1,0:T(8,128)(2,1)S(1)} custom-call(bf16[8,2,4,16,128]{4,3,2,1,0:T(8,128)(2,1)} %bitcast.5, bf16[1024,256]{1,0:T(8,128)(2,1)} %wq_in.1, bf16[1024,128]{1,0:T(8,128)(2,1)} %wl_in.1, f32[1,128]{1,0:T(1,128)} %bitcast.8, f32[1,128]{1,0:T(1,128)} %bitcast.9, bf16[2,64,128]{2,1,0:T(8,128)(2,1)} %bitcast.6, bf16[128,1024]{1,0:T(8,128)(2,1)} %w_in.1, ...), custom_call_target="tpu_custom_call" | custom-call | tf_op jit(solution)/shard_map/pallas_call | solution.py:563
  52.0 0.7 %copy.11 = bf16[1024,128]{1,0:T(8,128)(2,1)} copy(bf16[1024,128]{1,0:T(8,128)(2,1)S(1)} %shard_map.91) | data formatting | bytes 524288

commit v11 on v10

--- a/solution.py
+++ b/solution.py
@@ -52,7 +52,7 @@
         (16, 20, [(1, 9), (9, 15), (15, 20)]),
         (20, 24, [(1, 9), (17, 24), (9, 13), (13, 17)]),
         (24, 28, [(1, 9), (20, 28), (9, 15), (15, 20)]),
-        (28, 32, [(1, 9), (9, 17), (17, 25), (25, 32)]),
+        (28, 32, [(1, 7), (7, 13), (13, 19), (19, 24), (24, 29), (29, 32)]),
     ]
 
 
@@ -138,7 +138,7 @@
         return 2 * chip(i) + core
 
     def tokens_to(e, j):
-        c = lax.rem(core + e % 2, 2)
+        c = 1 - core if e == 1 else e % 2
         part = chip(e // 2 + j)
         return send(
             tok_ref.at[:, c, part], tk_ref.at[tp, part], (t_s.at[j], t_r.at[j]), at_tp(2 * chip(e // 2) + c)
@@ -179,7 +179,7 @@
         send(vu_ref, vus_ref, (c_s.at[1], c_r.at[1]), at_tp(sib)),
     ]
 
-    for e in (4, 5, 2, 3, 6, 7, 1):
+    for e in (5, 4, 3, 2, 7, 6, 1):
         tokens_to(e, 0).start()
     for d in range(1, kv_n):
 
@@ -378,15 +378,15 @@
 
         for g in range(1, count):
             spread_group(g)
-            if g <= 2:
-                pass_group(g - 1)
-        if count < 3:
-            pass_group(count - 1)
+            if g == 1:
+                pass_group(0)
+        if count < 2:
+            pass_group(0)
         for d in range(1, tp_n):
             weights_to(d).start()
         if not direct(0):
             relay_group(0)
-        passed, normed = min(count, 2), 0
+        passed, normed = 1, 0
         for j in range(1, xs):
             project(j)
         norm_group(normed)

time: 53.4 us -> 52.3 us (0.979)
  Pallas kernels: 52 us -> 51 us
    pallas_call x1, Pallas kernels: 52 us -> 51 us  [on_device(): pl.pallas_call(functools.partial(kernel, kv_n, tp_n), out_shape=jax.Shape...]
where the time goes in v11:
time: 52.3 us; the launch traced here: 51.7 us
  Pallas kernels  51 us (98%)
  local copies, waits for them, and re-layouts  0.71 us (1%)
    pallas_call x1, Pallas kernels, on_device(): pl.pallas_call(functools.partial(kernel, kv_n, tp_n), out_shape=jax.Shape...  51 us

profile of v11, /device:TPU:201, one launch (start us, length us, event | category | flops | bytes accessed | tf_op | source)
XLA Modules:
  0.0 51.7 jit_solution(6331918500429443449)
XLA Ops:
  0.0 51.0 %shard_map.91 = bf16[1024,128]{1,0:T(8,128)(2,1)S(1)} custom-call(bf16[8,2,4,16,128]{4,3,2,1,0:T(8,128)(2,1)} %bitcast.5, bf16[1024,256]{1,0:T(8,128)(2,1)} %wq_in.1, bf16[1024,128]{1,0:T(8,128)(2,1)} %wl_in.1, f32[1,128]{1,0:T(1,128)} %bitcast.8, f32[1,128]{1,0:T(1,128)} %bitcast.9, bf16[2,64,128]{2,1,0:T(8,128)(2,1)} %bitcast.6, bf16[128,1024]{1,0:T(8,128)(2,1)} %w_in.1, ...), custom_call_target="tpu_custom_call" | custom-call | tf_op jit(solution)/shard_map/pallas_call | solution.py:563
  51.0 0.7 %copy.11 = bf16[1024,128]{1,0:T(8,128)(2,1)} copy(bf16[1024,128]{1,0:T(8,128)(2,1)S(1)} %shard_map.91) | data formatting | bytes 524288

commit v12 on v11

--- a/solution.py
+++ b/solution.py
@@ -49,10 +49,10 @@
     return [
         (0, 8, [(1, 8)]),
         (8, 16, [(1, 7), (7, 12), (12, 16)]),
-        (16, 20, [(1, 9), (9, 15), (15, 20)]),
+        (16, 20, [(1, 7), (7, 11), (11, 15), (15, 18), (18, 20)]),
         (20, 24, [(1, 9), (17, 24), (9, 13), (13, 17)]),
-        (24, 28, [(1, 9), (20, 28), (9, 15), (15, 20)]),
-        (28, 32, [(1, 7), (7, 13), (13, 19), (19, 24), (24, 29), (29, 32)]),
+        (24, 28, [(1, 9), (20, 25), (25, 28), (9, 13), (13, 17), (17, 20)]),
+        (28, 32, [(1, 6), (6, 11), (11, 16), (16, 21), (21, 25), (25, 29), (29, 32)]),
     ]
 
 
@@ -347,7 +347,7 @@
                 arrived(kvp_ref.at[pl.ds(0, 4), pl.ds(*groups[g])], kr_r.at[g])
 
                 first, size = groups[g]
-                each = next(n for n in (4, 2, 1) if size % n == 0)
+                each = next(n for n in (6, 5, 4, 7, 3, 2, 1) if size % n == 0)
 
                 @pl.loop(0, size // each)
                 def _(i):

time: 52.3 us -> 51.6 us (0.987)
  Pallas kernels: 51 us -> 50.4 us
    pallas_call x1, Pallas kernels: 51 us -> 50.4 us  [on_device(): pl.pallas_call(functools.partial(kernel, kv_n, tp_n), out_shape=jax.Shape...]
where the time goes in v12:
time: 51.6 us; the launch traced here: 51.1 us
  Pallas kernels  50.4 us (98%)
  local copies, waits for them, and re-layouts  0.71 us (1%)
    pallas_call x1, Pallas kernels, on_device(): pl.pallas_call(functools.partial(kernel, kv_n, tp_n), out_shape=jax.Shape...  50.4 us

profile of v12, /device:TPU:201, one launch (start us, length us, event | category | flops | bytes accessed | tf_op | source)
XLA Modules:
  0.0 51.1 jit_solution(18044831091769025097)
XLA Ops:
  0.0 50.4 %shard_map.91 = bf16[1024,128]{1,0:T(8,128)(2,1)S(1)} custom-call(bf16[8,2,4,16,128]{4,3,2,1,0:T(8,128)(2,1)} %bitcast.5, bf16[1024,256]{1,0:T(8,128)(2,1)} %wq_in.1, bf16[1024,128]{1,0:T(8,128)(2,1)} %wl_in.1, f32[1,128]{1,0:T(1,128)} %bitcast.8, f32[1,128]{1,0:T(1,128)} %bitcast.9, bf16[2,64,128]{2,1,0:T(8,128)(2,1)} %bitcast.6, bf16[128,1024]{1,0:T(8,128)(2,1)} %w_in.1, ...), custom_call_target="tpu_custom_call" | custom-call | tf_op jit(solution)/shard_map/pallas_call | solution.py:563
  50.4 0.7 %copy.11 = bf16[1024,128]{1,0:T(8,128)(2,1)} copy(bf16[1024,128]{1,0:T(8,128)(2,1)S(1)} %shard_map.91) | data formatting | bytes 524288

commit v13 on v12

--- a/solution.py
+++ b/solution.py
@@ -190,8 +190,6 @@
     for j in range(1, xs):
         for e in beside:
             tokens_to(e, j).start()
-    for copy in to_sib:
-        copy.start()
     for p in range(xs):
         tk_ref[tp, p] = tok_ref[:, core, p]
     wc_ref[tp, y] = w_ref[
@@ -231,6 +229,8 @@
     pltpu.make_async_copy(map_ref, map_s, lc.at[0]).wait()
     to_smem.wait()
 
+    for copy in to_sib:
+        copy.start()
     def slots_of(d):
         return pl.ds(blocks + (d - 1) * PER_OWNER, PER_OWNER)
 
@@ -362,15 +362,15 @@
             when_group(g, body)
 
         spread_group(0)
+        count = len(groups)
+        for j in range(1, xs):
+            hand_tokens(j)
         for copy in to_sib:
             copy.wait()
         for v, at in ((vu_ref, core), (vus_ref, 1 - core)):
             for h in range(heads):
                 bd_ref[at, h * vdim : (h + 1) * vdim, h * width : (h + 1) * width] = v[h]
-        count = len(groups)
         project(0)
-        for j in range(1, xs):
-            hand_tokens(j)
         def weights_step():
             arrived(wc_ref.at[pl.ds(0, tp_n - 1), 0], w_r.at[0])
             for e in range(1, RING):

time: 51.6 us -> 51.6 us (level)
  no operation moved by 1% of the time
where the time goes in v13:
time: 51.6 us; the launch traced here: 51.2 us
  Pallas kernels  50.5 us (98%)
  local copies, waits for them, and re-layouts  0.71 us (1%)
    pallas_call x1, Pallas kernels, on_device(): pl.pallas_call(functools.partial(kernel, kv_n, tp_n), out_shape=jax.Shape...  50.5 us

profile of v13, /device:TPU:201, one launch (start us, length us, event | category | flops | bytes accessed | tf_op | source)
XLA Modules:
  0.0 51.2 jit_solution(5363935537049483621)
XLA Ops:
  0.0 50.5 %shard_map.91 = bf16[1024,128]{1,0:T(8,128)(2,1)S(1)} custom-call(bf16[8,2,4,16,128]{4,3,2,1,0:T(8,128)(2,1)} %bitcast.5, bf16[1024,256]{1,0:T(8,128)(2,1)} %wq_in.1, bf16[1024,128]{1,0:T(8,128)(2,1)} %wl_in.1, f32[1,128]{1,0:T(1,128)} %bitcast.8, f32[1,128]{1,0:T(1,128)} %bitcast.9, bf16[2,64,128]{2,1,0:T(8,128)(2,1)} %bitcast.6, bf16[128,1024]{1,0:T(8,128)(2,1)} %w_in.1, ...), custom_call_target="tpu_custom_call" | custom-call | tf_op jit(solution)/shard_map/pallas_call | solution.py:563
  50.5 0.7 %copy.11 = bf16[1024,128]{1,0:T(8,128)(2,1)} copy(bf16[1024,128]{1,0:T(8,128)(2,1)S(1)} %shard_map.91) | data formatting | bytes 524288

commit v14 on v13

--- a/solution.py
+++ b/solution.py
@@ -52,7 +52,7 @@
         (16, 20, [(1, 7), (7, 11), (11, 15), (15, 18), (18, 20)]),
         (20, 24, [(1, 9), (17, 24), (9, 13), (13, 17)]),
         (24, 28, [(1, 9), (20, 25), (25, 28), (9, 13), (13, 17), (17, 20)]),
-        (28, 32, [(1, 6), (6, 11), (11, 16), (16, 21), (21, 25), (25, 29), (29, 32)]),
+        (28, 32, [(1, 6), (6, 11), (11, 16), (16, 21), (21, 25), (25, 28), (28, 30), (30, 32)]),
     ]
 
 

time: 51.6 us -> 51.9 us (level)
  no operation moved by 1% of the time
where the time goes in v14:
time: 51.9 us; the launch traced here: 51.2 us
  Pallas kernels  50.5 us (97%)
  local copies, waits for them, and re-layouts  0.71 us (1%)
    pallas_call x1, Pallas kernels, on_device(): pl.pallas_call(functools.partial(kernel, kv_n, tp_n), out_shape=jax.Shape...  50.5 us

profile of v14, /device:TPU:201, one launch (start us, length us, event | category | flops | bytes accessed | tf_op | source)
XLA Modules:
  0.0 51.2 jit_solution(3416052451851642594)
XLA Ops:
  0.0 50.5 %shard_map.91 = bf16[1024,128]{1,0:T(8,128)(2,1)S(1)} custom-call(bf16[8,2,4,16,128]{4,3,2,1,0:T(8,128)(2,1)} %bitcast.5, bf16[1024,256]{1,0:T(8,128)(2,1)} %wq_in.1, bf16[1024,128]{1,0:T(8,128)(2,1)} %wl_in.1, f32[1,128]{1,0:T(1,128)} %bitcast.8, f32[1,128]{1,0:T(1,128)} %bitcast.9, bf16[2,64,128]{2,1,0:T(8,128)(2,1)} %bitcast.6, bf16[128,1024]{1,0:T(8,128)(2,1)} %w_in.1, ...), custom_call_target="tpu_custom_call" | custom-call | tf_op jit(solution)/shard_map/pallas_call | solution.py:563
  50.5 0.7 %copy.11 = bf16[1024,128]{1,0:T(8,128)(2,1)} copy(bf16[1024,128]{1,0:T(8,128)(2,1)S(1)} %shard_map.91) | data formatting | bytes 524288
